TPU v7x, 512 devices: a whole 4x4x16 slice. The times are simulated.
512 devices in a mesh: sp: 128 (over z, x, core), tp: 4 (over y).
Axes of the slice: x: 4, y: 4, z: 16, core: 2. Of those that a mesh axis runs over, the one named last changes fastest.
Arguments:
- tokens: bfloat16 [16384, 1024], P(('sp', 'tp')), may hold values from -13 to 13, as said below
- norm_gain: float32 [1024], replicated, may hold values from 0.5 to 1.5
- query_weight: bfloat16 [1024, 4096], P(None, 'tp'), may hold values from -0.1875 to 0.1875
- key_weight: bfloat16 [1024, 512], P(None, 'tp'), may hold values from -0.1875 to 0.1875
- value_weight: bfloat16 [1024, 512], P(None, 'tp'), may hold values from -0.1875 to 0.1875
- query_gain: float32 [128], replicated, may hold values from 0.5 to 1.5
- key_gain: float32 [128], replicated, may hold values from 0.5 to 1.5
- output_weight: bfloat16 [4096, 1024], P('tp'), may hold values from -1 to 1
Outputs:
- mixed: bfloat16 [16384, 1024], P(('sp', 'tp'))
Inputs may be any that keep to these rules, and one draw needn't show every extreme that they name: Every entry of tokens lies between -13 and 13.
All inputs are finite; a program needn't handle non-finite values.
Results may differ from a plain program's by a relative error of at most 0.015.
Values may be sent and summed in bfloat16 or wider, within the bound.
No kernel may reach another device: no remote copies, remote signals or barrier semaphores. Data moves between devices by JAX's collectives and lax.ppermute only.
A program may use at most 64 MiB of HBM per device.

v0:
```python
import math

import jax
import jax.numpy as jnp
import numpy as np
from jax import lax
from jax.experimental import pallas as pl
from jax.experimental.pallas import tpu as pltpu
from jax.sharding import Mesh, PartitionSpec as P


GRID_W = 64
EPS = 1e-06
BASE = 10000.0
HD = 128
TOK = 128
NZ, NX, NC, NY = 16, 4, 2, 4
KEY_SCALE, VALUE_SCALE = 2.0**11, 2.0**7
LROWS = 8
AROWS = HD + LROWS
PROWS = HD + 2 * LROWS
CHUNK = 512


def rotary_tables(grid_rows):
    axis_dim = HD // 2
    freq = np.power(np.float32(BASE), -np.arange(0, axis_dim, 2, dtype=np.float32) / np.float32(axis_dim))
    sign = np.tile(np.array([-1.0, 1.0]), axis_dim // 2)

    def half(count):
        angle = (np.arange(count, dtype=np.float32)[:, None] * freq[None, :].astype(np.float32)).astype(np.float64)
        angle = np.repeat(angle, 2, axis=1)
        return np.cos(angle), np.sin(angle) * sign

    row_cos, row_sin = half(grid_rows)
    col_cos, col_sin = half(GRID_W)
    pad_r, pad_c = np.ones_like(row_cos), np.ones_like(col_cos)
    rows = np.stack([np.concatenate([row_cos, pad_r], 1), np.concatenate([row_sin, pad_r], 1)])
    cols = np.stack([np.concatenate([pad_c, col_cos], 1), np.concatenate([pad_c, col_sin], 1)])
    return rows.astype(np.float32), cols.astype(np.float32)


VM = pl.BlockSpec(memory_space=pltpu.VMEM)


def call(kernel, shapes, *args, smem=0, flops=0, limit=24, alias=None):
    return pl.pallas_call(
        kernel,
        out_shape=shapes,
        in_specs=[pl.BlockSpec(memory_space=pltpu.SMEM)] * smem + [VM] * (len(args) - smem),
        out_specs=jax.tree.map(lambda s: VM, shapes),
        input_output_aliases=alias or {},
        cost_estimate=pl.CostEstimate(flops=flops, bytes_accessed=1 << 20, transcendentals=0),
        compiler_params=pltpu.CompilerParams(vmem_limit_bytes=limit << 20),
    )(*args)


def bf16(*shape):
    return jax.ShapeDtypeStruct(shape, jnp.bfloat16)


def f32(*shape):
    return jax.ShapeDtypeStruct(shape, jnp.float32)


def spread_kernel(tok_ref, out_ref, sems):
    copies = [pltpu.make_async_copy(tok_ref, out_ref.at[i], sems.at[i]) for i in range(NY)]
    for copy in copies:
        copy.start()
    for copy in copies:
        copy.wait()


def to_vmem(kernel, shapes, *args, count, limit=60):
    return pl.pallas_call(
        kernel,
        out_shape=shapes,
        in_specs=[pl.BlockSpec(memory_space=pltpu.HBM)] * len(args),
        out_specs=jax.tree.map(lambda s: VM, shapes),
        scratch_shapes=[pltpu.SemaphoreType.DMA((count,))],
        cost_estimate=pl.CostEstimate(flops=1 << 28, bytes_accessed=1 << 20, transcendentals=0),
        compiler_params=pltpu.CompilerParams(vmem_limit_bytes=limit << 20),
    )(*args)


def project_kernel(sp_ref, tok_ref, w_ref, vec_ref, rows_ref, cols_ref, q_ref, kv_ref):
    x = tok_ref[...].astype(jnp.float32)
    dim = x.shape[1]
    wide_q = w_ref.shape[1] - 2 * HD
    query_gain, key_gain = vec_ref[:, dim : dim + HD], vec_ref[:, dim + HD :]
    normed = x * lax.rsqrt(jnp.mean(x * x, axis=-1, keepdims=True) + EPS) * vec_ref[:, :dim]
    normed = normed.astype(jnp.bfloat16)
    first = sp_ref[0] * (TOK // GRID_W)

    def table(i):
        parts = [rows_ref[i, pl.ds(first + r, 1), :] * cols_ref[i] for r in range(TOK // GRID_W)]
        return jnp.concatenate(parts, axis=0)

    cosine, sine = table(0), table(1)
    even = lax.broadcasted_iota(jnp.int32, (TOK, HD), 1) % 2 == 0

    def turn(projected, gain):
        wide = projected.astype(jnp.bfloat16).astype(jnp.float32)
        wide = wide * lax.rsqrt(jnp.mean(wide * wide, axis=-1, keepdims=True) + EPS) * gain
        swapped = jnp.where(even, pltpu.roll(wide, HD - 1, 1), pltpu.roll(wide, 1, 1))
        return wide * cosine + swapped * sine

    keys = jnp.dot(normed, w_ref[:, wide_q : wide_q + HD], preferred_element_type=jnp.float32)
    keys = turn(keys, key_gain).astype(jnp.bfloat16)
    values = jnp.dot(normed, w_ref[:, wide_q + HD :], preferred_element_type=jnp.float32).T.astype(jnp.bfloat16)
    kv_ref[0] = keys
    kv_ref[1] = values
    queries = jnp.dot(normed, w_ref[:, :wide_q], preferred_element_type=jnp.float32)
    fold = HD ** (-0.5) * math.log2(math.e) / KEY_SCALE
    for h in range(queries.shape[1] // HD):
        turned = turn(queries[:, h * HD : (h + 1) * HD], query_gain) * fold
        turned = turned.T.astype(jnp.bfloat16)
        for i in range(NX):
            q_ref[i, :, h * TOK : (h + 1) * TOK] = turned


def pack(total):
    below = total[HD:]
    high = below.astype(jnp.bfloat16)
    low = (below - high.astype(jnp.float32)).astype(jnp.bfloat16)
    return jnp.concatenate([total[:HD].astype(jnp.bfloat16), high, low], axis=0)


def unpack(packed):
    wide = packed.astype(jnp.float32)
    return jnp.concatenate([wide[:HD], wide[HD:AROWS] + wide[AROWS:]], axis=0)


def fold_kernel(start, count, first, packed, q_ref, kv_ref, *refs):
    out_ref = refs[-1]
    ones = jnp.full((LROWS, CHUNK), VALUE_SCALE, jnp.bfloat16)
    per = CHUNK // TOK
    keys, values = [], []
    for j in range(start, start + count, per):
        keys.append(jnp.concatenate([kv_ref[i, 0] for i in range(j, j + per)], axis=0))
        columns = jnp.concatenate([kv_ref[i, 1] for i in range(j, j + per)], axis=1)
        values.append(jnp.concatenate([columns, ones], axis=0))
    for t in range(q_ref.shape[0]):
        q = q_ref[t]
        total = None if first else refs[0][t]
        for k, v in zip(keys, values):
            weights = jnp.exp2(jnp.dot(k, q, preferred_element_type=jnp.float32)).astype(jnp.bfloat16)
            part = jnp.dot(v, weights, preferred_element_type=jnp.float32)
            total = part if total is None else total + part
        out_ref[t] = pack(total) if packed else total


def fold(queries, blocks, start, count, acc, packed=False):
    nq, _, rows = queries.shape
    shape = bf16(nq, PROWS, rows) if packed else f32(nq, AROWS, rows)

    def kernel(*refs):
        fold_kernel(start, count, acc is None, packed, *refs)

    args = (queries, blocks) + (() if acc is None else (acc,))
    alias = {} if acc is None or packed else {2: 0}
    return call(kernel, shape, *args, flops=4 * nq * rows * count * TOK * HD, alias=alias)


def merge_kernel(acc_ref, other_ref, out_ref):
    for t in range(acc_ref.shape[0]):
        out_ref[t] = pack(acc_ref[t] + unpack(other_ref[t]))


def finish_kernel(part_ref, w_ref, out_ref):
    total = unpack(part_ref[0])
    for t in range(1, part_ref.shape[0]):
        total = total + unpack(part_ref[t])
    quotient = total[:HD] * (1.0 / total[HD : HD + 1])
    heads = [quotient[:, i : i + TOK].T.astype(jnp.bfloat16) for i in range(0, quotient.shape[1], TOK)]
    attended = jnp.concatenate(heads, axis=1)
    out_ref[...] = jnp.dot(attended, w_ref[...], preferred_element_type=jnp.float32).astype(jnp.bfloat16)


def sum_kernel(part_ref, out_ref):
    total = part_ref[0].astype(jnp.float32)
    for p in range(1, part_ref.shape[0]):
        total = total + part_ref[p].astype(jnp.float32)
    out_ref[...] = total.astype(out_ref.dtype)


def per_device(tables, tokens, norm_gain, wq, wk, wv, query_gain, key_gain, wo):
    z, x, c = (lax.axis_index(a) for a in ("z", "x", "c"))
    sp = (z * NX + x) * NC + c
    rows, dim = tokens.shape
    width = wq.shape[1]
    copies = to_vmem(spread_kernel, bf16(NY, rows, dim), tokens, count=NY)
    mine = lax.all_to_all(copies, "y", 0, 0, tiled=True).reshape(NY * rows, dim)
    weights = jnp.concatenate([wq, wk, wv], axis=1)
    gains = jnp.concatenate([norm_gain, query_gain, key_gain]).reshape(1, -1)
    q, kv = call(
        project_kernel,
        (bf16(NX, HD, width), bf16(2, TOK, HD)),
        jnp.reshape(sp, (1,)).astype(jnp.int32),
        mine,
        weights,
        gains,
        *tables,
        smem=1,
        flops=2 * TOK * 1024 * 1280,
    )
    own_q = lax.all_to_all(q, "x", 0, 0, tiled=True)
    scaled = jnp.concatenate([kv[:1] * KEY_SCALE, kv[1:] * VALUE_SCALE]).astype(jnp.float16)
    gathered = lax.all_gather(scaled[None], "z", axis=0, tiled=True)
    other_q = lax.ppermute(own_q, "c", [(0, 1), (1, 0)])
    blocks = gathered.astype(jnp.bfloat16)
    half = NZ // 2
    own = fold(own_q, blocks, 0, half, None)
    other = fold(other_q, blocks, 0, half, None)
    other = fold(other_q, blocks, half, half, other, packed=True)
    arrived = lax.ppermute(other, "c", [(0, 1), (1, 0)])
    own = fold(own_q, blocks, half, half, own)
    merged = call(merge_kernel, bf16(NX, PROWS, width), own, arrived)
    parts = lax.all_to_all(merged, "x", 0, 0, tiled=True)
    mixed = call(finish_kernel, bf16(TOK, wo.shape[1]), parts, wo, flops=2 * TOK * 1024 * 1024)
    shares = lax.all_to_all(mixed.reshape(NY, rows, -1), "y", 0, 0, tiled=True)
    return call(sum_kernel, bf16(rows, dim), shares)


def solution(mesh):
    fine = Mesh(mesh.devices.reshape(NZ, NX, NC, NY), ("z", "x", "c", "y"))
    sp = ("z", "x", "c")
    tables = rotary_tables(NZ * NX * NC * TOK // GRID_W)

    def run(*args):
        return per_device(tables, *args)

    return jax.shard_map(
        run,
        mesh=fine,
        in_specs=(
            P(sp + ("y",), None),
            P(),
            P(None, "y"),
            P(None, "y"),
            P(None, "y"),
            P(),
            P(),
            P("y", None),
        ),
        out_specs=P(sp + ("y",), None),
        check_vma=False,
    )
```

profile of v0, /device:TPU:1, one launch (start us, length us, event | category | flops | bytes accessed | tf_op | source)
XLA Modules:
  0.0 122.6 jit_solution(17133425943863010666)
XLA Ops:
  0.0 1.7 %shard_map.100 = bf16[4,32,1024]{2,1,0:T(8,128)(2,1)} custom-call(bf16[32,1024]{1,0:T(8,128)(2,1)} %tok_ref.1), custom_call_target="tpu_custom_call" | custom-call | flops 268435456 | bytes 1048576 | tf_op jit(solution)/shard_map/pallas_call | solution.py:75
  1.7 5.0 %all-to-all-start = ((bf16[4,32,1024]{2,1,0:T(8,128)(2,1)}), bf16[4,32,1024]{2,1,0:T(8,128)(2,1)S(1)}, u32[]{:S(2)}, u32[]{:S(2)}) async-start(bf16[4,32,1024]{2,1,0:T(8,128)(2,1)} %shard_map.100), calls=%async_computation | async-start | bytes 524288 | tf_op jit(solution)/shard_map/all_to_all | solution.py:193
  6.7 0.7 pad_maximum_fusion.1
  7.5 0.0 copy-start.1
  7.5 0.0 copy-start.2
  7.5 2.1 %pad_maximum_fusion.w_ref = bf16[1024,1280]{1,0:T(8,128)(2,1)S(1)} fusion(bf16[1024,128]{1,0:T(8,128)(2,1)} %param.14, bf16[1024,128]{1,0:T(8,128)(2,1)} %param.13, bf16[1024,1024]{1,0:T(8,128)(2,1)} %param.12), kind=kLoop, calls=%fused_computation | loop fusion | flops 7864320 | bytes 5242880 | tf_op jit(solution)/shard_map/concatenate | solution.py:194
  9.6 2.7 %all-to-all-done = bf16[4,32,1024]{2,1,0:T(8,128)(2,1)S(1)} async-done(((bf16[4,32,1024]{2,1,0:T(8,128)(2,1)}), bf16[4,32,1024]{2,1,0:T(8,128)(2,1)S(1)}, u32[]{:S(2)}, u32[]{:S(2)}) %all-to-all-start) | async-done | bytes 262176 | tf_op jit(solution)/shard_map/all_to_all | solution.py:193
  12.3 1.6 %shard_map.101 = (bf16[4,128,1024]{2,1,0:T(8,128)(2,1)S(1)}, bf16[2,128,128]{2,1,0:T(8,128)(2,1)S(1)}) custom-call(s32[1]{0:T(128)} %bitcast.sp_ref, bf16[128,1024]{1,0:T(8,128)(2,1)S(1)} %bitcast.7, bf16[1024,1280]{1,0:T(8,128)(2,1)S(1)} %pad_maximum_fusion.w_ref, f32[1,1280]{1,0:T(1,128)S(1)} %reshape.43.vec_ref, f32[2,256,128]{2,1,0:T(8,128)S(1)} %copy-done.1, ...), custom_call_target="tpu_custom_call" | custom-call | flops 335544320 | bytes 1048576 | tf_op jit(solution)/shard_map/pallas_call | solution.py:47
  13.9 13.8 %all_to_all.20.refs_0_ = bf16[4,128,1024]{2,1,0:T(8,128)(2,1)S(1)} all-to-all(bf16[4,128,1024]{2,1,0:T(8,128)(2,1)S(1)} %get-tuple-element.7), channel_id=1, replica_groups=mesh['z'=16,'x'=4,'c'=2,'y'=4] {'x'}, dimensions={0} | all-to-all | bytes 2097152 | tf_op jit(solution)/shard_map/all_to_all | solution.py:207
  27.7 8.0 %collective-permute-start = (bf16[4,128,1024]{2,1,0:T(8,128)(2,1)S(1)}, bf16[4,128,1024]{2,1,0:T(8,128)(2,1)S(1)}, u32[]{:S(2)}, u32[]{:S(2)}) collective-permute-start(bf16[4,128,1024]{2,1,0:T(8,128)(2,1)S(1)} %all_to_all.20.refs_0_), channel_id=1, source_target_pairs={{0,4},{4,0},{1,5},{5,1},{2,6},{6,2},{3,7},{7,3},{8,12},{12,8},{9,1... | collective-permute-start | bytes 3145736 | tf_op jit(solution)/shard_map/ppermute | solution.py:210
  35.7 35.6 %all-gather.1 = f16[16,2,128,128]{3,2,1,0:T(8,128)(2,1)S(1)} all-gather(f16[1,2,128,128]{3,2,1,0:T(8,128)(2,1)S(1)} %maximum_convert_fusion), channel_id=1, replica_groups=mesh['z'=16,'x'=4,'c'=2,'y'=4] {'z'}, dimensions={0}, use_global_device_ids=true | all-gather | bytes 1114112 | tf_op jit(solution)/shard_map/all_gather | solution.py:209
  71.3 0.2 convert_element_type.14.refs_1_
  71.5 0.0 collective-permute-done.refs_0_
  71.5 3.6 %shard_map.104.refs_2_ = f32[4,136,1024]{2,1,0:T(8,128)S(1)} custom-call(bf16[4,128,1024]{2,1,0:T(8,128)(2,1)S(1)} %collective-permute-done.refs_0_, bf16[16,2,128,128]{3,2,1,0:T(8,128)(2,1)S(1)} %convert_element_type.14.refs_1_), custom_call_target="tpu_custom_call" | custom-call | flops 2147483648 | bytes 1048576 | tf_op jit(solution)/shard_map/pallas_call | solution.py:47
  75.1 3.6 %shard_map.105 = bf16[4,144,1024]{2,1,0:T(8,128)(2,1)S(1)} custom-call(bf16[4,128,1024]{2,1,0:T(8,128)(2,1)S(1)} %collective-permute-done.refs_0_, bf16[16,2,128,128]{3,2,1,0:T(8,128)(2,1)S(1)} %convert_element_type.14.refs_1_, f32[4,136,1024]{2,1,0:T(8,128)S(1)} %shard_map.104.refs_2_), custom_call_target="tpu_custom_call" | custom-call | flops 2147483648 | bytes 1048576 | tf_op jit(solution)/shard_map/pallas_call | solution.py:47
  78.7 8.3 %collective-permute-start.1 = (bf16[4,144,1024]{2,1,0:T(8,128)(2,1)S(1)}, bf16[4,144,1024]{2,1,0:T(8,128)(2,1)S(1)}, u32[]{:S(2)}, u32[]{:S(2)}) collective-permute-start(bf16[4,144,1024]{2,1,0:T(8,128)(2,1)S(1)} %shard_map.105), channel_id=1, source_target_pairs={{0,4},{4,0},{1,5},{5,1},{2,6},{6,2},{3,7},{7,3},{8,12},{12,8},{9,1... | collective-permute-start | bytes 3538952 | tf_op jit(solution)/shard_map/ppermute | solution.py:216
  87.0 3.6 %shard_map.102.refs_2_ = f32[4,136,1024]{2,1,0:T(8,128)S(1)} custom-call(bf16[4,128,1024]{2,1,0:T(8,128)(2,1)S(1)} %all_to_all.20.refs_0_, bf16[16,2,128,128]{3,2,1,0:T(8,128)(2,1)S(1)} %convert_element_type.14.refs_1_), custom_call_target="tpu_custom_call" | custom-call | flops 2147483648 | bytes 1048576 | tf_op jit(solution)/shard_map/pallas_call | solution.py:47
  90.5 3.8 %shard_map.103.acc_ref = f32[4,136,1024]{2,1,0:T(8,128)S(1)} custom-call(bf16[4,128,1024]{2,1,0:T(8,128)(2,1)S(1)} %all_to_all.20.refs_0_, bf16[16,2,128,128]{3,2,1,0:T(8,128)(2,1)S(1)} %convert_element_type.14.refs_1_, f32[4,136,1024]{2,1,0:T(8,128)S(1)} %shard_map.102.refs_2_), custom_call_target="tpu_custom_call", output_to_operand_aliasing={{}: (2, {})} | custom-call | flops 2147483648 | bytes 1048576 | tf_op jit(solution)/shard_map/pallas_call | solution.py:47
  94.3 0.0 copy-start
  94.4 0.2 shard_map.106
  94.6 18.8 %all_to_all.21.part_ref = bf16[4,144,1024]{2,1,0:T(8,128)(2,1)S(1)} all-to-all(bf16[4,144,1024]{2,1,0:T(8,128)(2,1)S(1)} %shard_map.106), channel_id=1, replica_groups=mesh['z'=16,'x'=4,'c'=2,'y'=4] {'x'}, dimensions={0} | all-to-all | bytes 2359296 | tf_op jit(solution)/shard_map/all_to_all | solution.py:219
  113.4 0.5 shard_map.107
  114.0 7.9 %all_to_all.22.part_ref = bf16[4,32,1024]{2,1,0:T(8,128)(2,1)S(1)} all-to-all(bf16[4,32,1024]{2,1,0:T(8,128)(2,1)S(1)} %bitcast.8), channel_id=1, replica_groups=mesh['z'=16,'x'=4,'c'=2,'y'=4] {'y'}, dimensions={0} | all-to-all | bytes 524288 | tf_op jit(solution)/shard_map/all_to_all | solution.py:221
  121.9 0.7 shard_map.108
  (7 shorter events, 0.0 us)
Async XLA Ops:
  1.7 10.5 %all-to-all-start = ((bf16[4,32,1024]{2,1,0:T(8,128)(2,1)}), bf16[4,32,1024]{2,1,0:T(8,128)(2,1)S(1)}, u32[]{:S(2)}, u32[]{:S(2)}) async-start(bf16[4,32,1024]{2,1,0:T(8,128)(2,1)} %shard_map.100), calls=%async_computation | async-start | bytes 524288 | tf_op jit(solution)/shard_map/all_to_all | solution.py:193
  7.5 4.8 %copy-start.1 = (f32[2,256,128]{2,1,0:T(8,128)S(1)}, f32[2,256,128]{2,1,0:T(8,128)}, u32[]{:S(2)}) copy-start(f32[2,256,128]{2,1,0:T(8,128)} %constant.28.clone.rows_ref) | copy-start | bytes 786436
  7.5 4.8 %copy-start.2 = (f32[2,64,128]{2,1,0:T(8,128)S(1)}, f32[2,64,128]{2,1,0:T(8,128)}, u32[]{:S(2)}) copy-start(f32[2,64,128]{2,1,0:T(8,128)} %constant.29.clone.cols_ref) | copy-start | bytes 196612
  27.7 43.8 %collective-permute-start = (bf16[4,128,1024]{2,1,0:T(8,128)(2,1)S(1)}, bf16[4,128,1024]{2,1,0:T(8,128)(2,1)S(1)}, u32[]{:S(2)}, u32[]{:S(2)}) collective-permute-start(bf16[4,128,1024]{2,1,0:T(8,128)(2,1)S(1)} %all_to_all.20.refs_0_), channel_id=1, source_target_pairs={{0,4},{4,0},{1,5},{5,1},{2,6},{6,2},{3,7},{7,3},{8,12},{12,8},{9,1... | collective-permute-start | bytes 3145736 | tf_op jit(solution)/shard_map/ppermute | solution.py:210
  78.7 15.7 %collective-permute-start.1 = (bf16[4,144,1024]{2,1,0:T(8,128)(2,1)S(1)}, bf16[4,144,1024]{2,1,0:T(8,128)(2,1)S(1)}, u32[]{:S(2)}, u32[]{:S(2)}) collective-permute-start(bf16[4,144,1024]{2,1,0:T(8,128)(2,1)S(1)} %shard_map.105), channel_id=1, source_target_pairs={{0,4},{4,0},{1,5},{5,1},{2,6},{6,2},{3,7},{7,3},{8,12},{12,8},{9,1... | collective-permute-start | bytes 3538952 | tf_op jit(solution)/shard_map/ppermute | solution.py:216
  94.3 19.1 %copy-start = (bf16[1024,1024]{1,0:T(8,128)(2,1)S(1)}, bf16[1024,1024]{1,0:T(8,128)(2,1)}, u32[]{:S(2)}) copy-start(bf16[1024,1024]{1,0:T(8,128)(2,1)} %w_ref.1) | copy-start | bytes 6291460
where the time goes:
time: 123 us
  blocking collectives  76.1 us (62%)
  starting transfers between devices  21.3 us (17%)
  Pallas kernels  19.2 us (16%)
  other arithmetic  3.01 us (2%)
  waiting for transfers between devices  2.71 us (2%)
    all_gather x1, blocking collectives, per_device(): gathered = lax.all_gather(scaled[None], 'z', axis=0, tiled=True)  35.6 us
    all_to_all x1, blocking collectives, per_device(): parts = lax.all_to_all(merged, 'x', 0, 0, tiled=True)  18.8 us
    pallas_call x8, Pallas kernels, call(): pl.pallas_call(kernel, out_shape=shapes, in_specs=[pl.BlockSpec(memory_sp...  17.5 us
    all_to_all x1, blocking collectives, per_device(): own_q = lax.all_to_all(q, 'x', 0, 0, tiled=True)  13.8 us
    ppermute x1, starting transfers between devices, per_device(): arrived = lax.ppermute(other, 'c', [(0, 1), (1, 0)])  8.3 us
    ppermute x1, starting transfers between devices, per_device(): other_q = lax.ppermute(own_q, 'c', [(0, 1), (1, 0)])  8 us
    all_to_all x1, blocking collectives, per_device(): shares = lax.all_to_all(mixed.reshape(NY, rows, -1), 'y', 0, 0, tiled=True)  7.92 us
    all_to_all x1, starting transfers between devices, per_device(): mine = lax.all_to_all(copies, 'y', 0, 0, tiled=True).reshape(NY * rows, dim)  5.01 us
  transfers between devices with their start and end apart: 3, of which 1 were waited for; matrix products, arithmetic and copies ran while one was open for 2% of the time, Pallas kernels for 6%

commit v1 on v0

--- a/solution.py
+++ b/solution.py
@@ -18,7 +18,8 @@
 KEY_SCALE, VALUE_SCALE = 2.0**11, 2.0**7
 LROWS = 8
 AROWS = HD + LROWS
-PROWS = HD + 2 * LROWS
+PROWS = HD + LROWS
+RINGS = [[i * NC + (i + g) % NC for i in range(NZ)] for g in range(NC)]
 CHUNK = 512
 
 
@@ -71,19 +72,18 @@
         copy.wait()
 
 
-def to_vmem(kernel, shapes, *args, count, limit=60):
+def spread(array, count):
     return pl.pallas_call(
-        kernel,
-        out_shape=shapes,
-        in_specs=[pl.BlockSpec(memory_space=pltpu.HBM)] * len(args),
-        out_specs=jax.tree.map(lambda s: VM, shapes),
+        spread_kernel,
+        out_shape=jax.ShapeDtypeStruct((count,) + array.shape, array.dtype),
+        in_specs=[VM],
+        out_specs=pl.BlockSpec(memory_space=pltpu.HBM),
         scratch_shapes=[pltpu.SemaphoreType.DMA((count,))],
-        cost_estimate=pl.CostEstimate(flops=1 << 28, bytes_accessed=1 << 20, transcendentals=0),
-        compiler_params=pltpu.CompilerParams(vmem_limit_bytes=limit << 20),
-    )(*args)
-
-
-def project_kernel(sp_ref, tok_ref, w_ref, vec_ref, rows_ref, cols_ref, q_ref, kv_ref):
+        name="spread",
+    )(array)
+
+
+def project_kernel(sp_ref, tok_ref, w_ref, vec_ref, rows_ref, cols_ref, q_ref, kv_ref, turned_ref, sems):
     x = tok_ref[...].astype(jnp.float32)
     dim = x.shape[1]
     wide_q = w_ref.shape[1] - 2 * HD
@@ -106,71 +106,71 @@
         return wide * cosine + swapped * sine
 
     keys = jnp.dot(normed, w_ref[:, wide_q : wide_q + HD], preferred_element_type=jnp.float32)
-    keys = turn(keys, key_gain).astype(jnp.bfloat16)
-    values = jnp.dot(normed, w_ref[:, wide_q + HD :], preferred_element_type=jnp.float32).T.astype(jnp.bfloat16)
+    keys = turn(keys, key_gain).astype(jnp.bfloat16) * KEY_SCALE
+    values = jnp.dot(normed, w_ref[:, wide_q + HD :], preferred_element_type=jnp.float32).T.astype(jnp.bfloat16) * VALUE_SCALE
     kv_ref[0] = keys
     kv_ref[1] = values
     queries = jnp.dot(normed, w_ref[:, :wide_q], preferred_element_type=jnp.float32)
     fold = HD ** (-0.5) * math.log2(math.e) / KEY_SCALE
     for h in range(queries.shape[1] // HD):
         turned = turn(queries[:, h * HD : (h + 1) * HD], query_gain) * fold
-        turned = turned.T.astype(jnp.bfloat16)
-        for i in range(NX):
-            q_ref[i, :, h * TOK : (h + 1) * TOK] = turned
+        turned_ref[:, h * TOK : (h + 1) * TOK] = turned.T.astype(jnp.bfloat16)
+    copies = [pltpu.make_async_copy(turned_ref, q_ref.at[i], sems.at[i]) for i in range(NX)]
+    for copy in copies:
+        copy.start()
+    for copy in copies:
+        copy.wait()
 
 
 def pack(total):
     below = total[HD:]
-    high = below.astype(jnp.bfloat16)
-    low = (below - high.astype(jnp.float32)).astype(jnp.bfloat16)
-    return jnp.concatenate([total[:HD].astype(jnp.bfloat16), high, low], axis=0)
+    high = below.astype(jnp.bfloat16).astype(jnp.float32)
+    odd = lax.broadcasted_iota(jnp.int32, below.shape, 0) % 2 == 1
+    return jnp.concatenate([total[:HD], jnp.where(odd, below - high, high)], axis=0).astype(jnp.bfloat16)
 
 
 def unpack(packed):
     wide = packed.astype(jnp.float32)
-    return jnp.concatenate([wide[:HD], wide[HD:AROWS] + wide[AROWS:]], axis=0)
-
-
-def fold_kernel(start, count, first, packed, q_ref, kv_ref, *refs):
-    out_ref = refs[-1]
+    return jnp.concatenate([wide[:HD], wide[HD : HD + 1] + wide[HD + 1 : HD + 2]], axis=0)
+
+
+def fold_kernel(tiles, sets, resumed, packed, at_ref, q_ref, *refs):
+    kv_refs, sum_refs, out_refs = refs[:sets], refs[sets : len(refs) - tiles], refs[len(refs) - tiles :]
     ones = jnp.full((LROWS, CHUNK), VALUE_SCALE, jnp.bfloat16)
     per = CHUNK // TOK
     keys, values = [], []
-    for j in range(start, start + count, per):
-        keys.append(jnp.concatenate([kv_ref[i, 0] for i in range(j, j + per)], axis=0))
-        columns = jnp.concatenate([kv_ref[i, 1] for i in range(j, j + per)], axis=1)
-        values.append(jnp.concatenate([columns, ones], axis=0))
-    for t in range(q_ref.shape[0]):
-        q = q_ref[t]
-        total = None if first else refs[0][t]
+    for kv_ref in kv_refs:
+        for j in range(0, kv_ref.shape[0], per):
+            keys.append(jnp.concatenate([kv_ref[i, 0] for i in range(j, j + per)], axis=0))
+            columns = jnp.concatenate([kv_ref[i, 1] for i in range(j, j + per)], axis=1)
+            values.append(jnp.concatenate([columns, ones], axis=0))
+    for t in range(tiles):
+        q = q_ref[at_ref[t]]
+        total = sum_refs[t][...] if resumed else None
         for k, v in zip(keys, values):
             weights = jnp.exp2(jnp.dot(k, q, preferred_element_type=jnp.float32)).astype(jnp.bfloat16)
             part = jnp.dot(v, weights, preferred_element_type=jnp.float32)
             total = part if total is None else total + part
-        out_ref[t] = pack(total) if packed else total
-
-
-def fold(queries, blocks, start, count, acc, packed=False):
-    nq, _, rows = queries.shape
-    shape = bf16(nq, PROWS, rows) if packed else f32(nq, AROWS, rows)
+        out_refs[t][...] = pack(total) if packed else total
+
+
+def fold(at, queries, blocks, sums=(), packed=False):
+    tiles = at.shape[0]
+    width = queries.shape[2]
+    shape = tuple(bf16(PROWS, width) if packed else f32(AROWS, width) for _ in range(tiles))
 
     def kernel(*refs):
-        fold_kernel(start, count, acc is None, packed, *refs)
-
-    args = (queries, blocks) + (() if acc is None else (acc,))
-    alias = {} if acc is None or packed else {2: 0}
-    return call(kernel, shape, *args, flops=4 * nq * rows * count * TOK * HD, alias=alias)
-
-
-def merge_kernel(acc_ref, other_ref, out_ref):
-    for t in range(acc_ref.shape[0]):
-        out_ref[t] = pack(acc_ref[t] + unpack(other_ref[t]))
-
-
-def finish_kernel(part_ref, w_ref, out_ref):
-    total = unpack(part_ref[0])
-    for t in range(1, part_ref.shape[0]):
-        total = total + unpack(part_ref[t])
+        fold_kernel(tiles, len(blocks), len(sums) > 0, packed, *refs)
+
+    flops = 4 * tiles * width * sum(b.shape[0] for b in blocks) * TOK * HD
+    return call(kernel, shape, at, queries, *blocks, *sums, smem=1, flops=flops)
+
+
+def finish_kernel(own_ref, *refs):
+    part_refs, w_ref, out_ref = refs[:-2], refs[-2], refs[-1]
+    total = own_ref[: HD + 1]
+    for part_ref in part_refs:
+        total = total + unpack(part_ref[...])
     quotient = total[:HD] * (1.0 / total[HD : HD + 1])
     heads = [quotient[:, i : i + TOK].T.astype(jnp.bfloat16) for i in range(0, quotient.shape[1], TOK)]
     attended = jnp.concatenate(heads, axis=1)
@@ -189,35 +189,39 @@
     sp = (z * NX + x) * NC + c
     rows, dim = tokens.shape
     width = wq.shape[1]
-    copies = to_vmem(spread_kernel, bf16(NY, rows, dim), tokens, count=NY)
+    copies = spread(tokens, NY)
     mine = lax.all_to_all(copies, "y", 0, 0, tiled=True).reshape(NY * rows, dim)
     weights = jnp.concatenate([wq, wk, wv], axis=1)
     gains = jnp.concatenate([norm_gain, query_gain, key_gain]).reshape(1, -1)
-    q, kv = call(
+    q, kv = pl.pallas_call(
         project_kernel,
-        (bf16(NX, HD, width), bf16(2, TOK, HD)),
-        jnp.reshape(sp, (1,)).astype(jnp.int32),
-        mine,
-        weights,
-        gains,
-        *tables,
-        smem=1,
-        flops=2 * TOK * 1024 * 1280,
-    )
+        out_shape=(bf16(NX, HD, width), bf16(2, TOK, HD)),
+        in_specs=[pl.BlockSpec(memory_space=pltpu.SMEM)] + [VM] * 5,
+        out_specs=(pl.BlockSpec(memory_space=pltpu.HBM), VM),
+        scratch_shapes=[pltpu.VMEM((HD, width), jnp.bfloat16), pltpu.SemaphoreType.DMA((NX,))],
+        name="project",
+        cost_estimate=pl.CostEstimate(flops=2 * TOK * dim * (width + 2 * HD), bytes_accessed=1 << 20, transcendentals=0),
+        compiler_params=pltpu.CompilerParams(vmem_limit_bytes=24 << 20),
+    )(jnp.reshape(sp, (1,)).astype(jnp.int32), mine, weights, gains, *tables)
     own_q = lax.all_to_all(q, "x", 0, 0, tiled=True)
-    scaled = jnp.concatenate([kv[:1] * KEY_SCALE, kv[1:] * VALUE_SCALE]).astype(jnp.float16)
-    gathered = lax.all_gather(scaled[None], "z", axis=0, tiled=True)
-    other_q = lax.ppermute(own_q, "c", [(0, 1), (1, 0)])
+    scaled = kv.astype(jnp.float16)
+    gathered = lax.all_gather(scaled[None], ("z", "c"), axis_index_groups=RINGS, axis=0, tiled=True)
     blocks = gathered.astype(jnp.bfloat16)
-    half = NZ // 2
-    own = fold(own_q, blocks, 0, half, None)
-    other = fold(other_q, blocks, 0, half, None)
-    other = fold(other_q, blocks, half, half, other, packed=True)
-    arrived = lax.ppermute(other, "c", [(0, 1), (1, 0)])
-    own = fold(own_q, blocks, half, half, own)
-    merged = call(merge_kernel, bf16(NX, PROWS, width), own, arrived)
-    parts = lax.all_to_all(merged, "x", 0, 0, tiled=True)
-    mixed = call(finish_kernel, bf16(TOK, wo.shape[1]), parts, wo, flops=2 * TOK * 1024 * 1024)
+    others = lax.ppermute(blocks, "c", [(0, 1), (1, 0)])
+    at = [jnp.reshape((x + d) % NX, (1,)).astype(jnp.int32) for d in range(NX)]
+
+    def send(block, d):
+        return lax.ppermute(block, "x", [(i, (i + d) % NX) for i in range(NX)])
+
+    (two,) = fold(at[2], own_q, (blocks,))
+    (two,) = fold(at[2], own_q, (others,), (two,), packed=True)
+    two = send(two, 2)
+    (one,) = fold(at[1], own_q, (blocks, others), packed=True)
+    one = send(one, 1)
+    (three,) = fold(at[3], own_q, (blocks, others), packed=True)
+    three = send(three, 3)
+    (kept,) = fold(at[0], own_q, (blocks, others))
+    mixed = call(finish_kernel, bf16(TOK, wo.shape[1]), kept, two, one, three, wo, flops=2 * TOK * 1024 * 1024)
     shares = lax.all_to_all(mixed.reshape(NY, rows, -1), "y", 0, 0, tiled=True)
     return call(sum_kernel, bf16(rows, dim), shares)
 

time: 123 us -> 117 us (0.951)
  the two profiles are of different devices: /device:TPU:1 before, /device:TPU:32 now
where the time goes in v1:
time: 117 us
  blocking collectives  47.4 us (41%)
  waiting for transfers between devices  23.4 us (20%)
  Pallas kernels  20.4 us (17%)
  starting transfers between devices  19.9 us (17%)
  other arithmetic  3.1 us (3%)
  local copies, waits for them, and re-layouts  2.47 us (2%)
    all_gather x1, blocking collectives, per_device(): lax.all_gather(scaled[None], ('z', 'c'), axis_index_groups=RINGS, axis=0,...  38.3 us
    pallas_call x7, Pallas kernels, call(): pl.pallas_call(kernel, out_shape=shapes, in_specs=[pl.BlockSpec(memory_sp...  17.2 us
    all_to_all x1, waiting for transfers between devices, per_device(): own_q = lax.all_to_all(q, 'x', 0, 0, tiled=True)  15.7 us
    ppermute x3, starting transfers between devices, send(): return lax.ppermute(block, 'x', [(i, (i + d) % NX) for i in range(NX)])  9.13 us
    all_to_all x1, blocking collectives, per_device(): shares = lax.all_to_all(mixed.reshape(NY, rows, -1), 'y', 0, 0, tiled=True)  9.07 us
    all_to_all x1, starting transfers between devices, per_device(): mine = lax.all_to_all(copies, 'y', 0, 0, tiled=True).reshape(NY * rows, dim)  4.48 us
    all_to_all x1, starting transfers between devices, per_device(): own_q = lax.all_to_all(q, 'x', 0, 0, tiled=True)  4.31 us
    ppermute x3, waiting for transfers between devices, send(): return lax.ppermute(block, 'x', [(i, (i + d) % NX) for i in range(NX)])  3.87 us
  transfers between devices with their start and end apart: 6, of which 4 were waited for; matrix products, arithmetic and copies ran while one was open for 2% of the time, Pallas kernels for 10%

profile of v1, /device:TPU:32, one launch (start us, length us, event | category | flops | bytes accessed | tf_op | source)
XLA Modules:
  0.0 116.9 jit_solution(766167730065146212)
XLA Ops:
  0.0 1.6 %spread.1 = bf16[4,32,1024]{2,1,0:T(8,128)(2,1)} custom-call(bf16[32,1024]{1,0:T(8,128)(2,1)} %tok_ref.1), custom_call_target="tpu_custom_call" | custom-call | tf_op jit(solution)/shard_map/spread/pallas_call | solution.py:76
  1.6 4.5 %all-to-all-start = ((bf16[4,32,1024]{2,1,0:T(8,128)(2,1)}), bf16[4,32,1024]{2,1,0:T(8,128)(2,1)S(1)}, u32[]{:S(2)}, u32[]{:S(2)}) async-start(bf16[4,32,1024]{2,1,0:T(8,128)(2,1)} %spread.1), calls=%async_computation | async-start | bytes 524288 | tf_op jit(solution)/shard_map/all_to_all | solution.py:193
  6.1 0.7 pad_maximum_fusion.1
  6.8 2.1 %pad_maximum_fusion.w_ref = bf16[1024,1280]{1,0:T(8,128)(2,1)S(1)} fusion(bf16[1024,128]{1,0:T(8,128)(2,1)} %param.14, bf16[1024,128]{1,0:T(8,128)(2,1)} %param.13, bf16[1024,1024]{1,0:T(8,128)(2,1)} %param.12), kind=kLoop, calls=%fused_computation | loop fusion | flops 7864320 | bytes 5242880 | tf_op jit(solution)/shard_map/concatenate | solution.py:194
  8.9 3.9 %all-to-all-done = bf16[4,32,1024]{2,1,0:T(8,128)(2,1)S(1)} async-done(((bf16[4,32,1024]{2,1,0:T(8,128)(2,1)}), bf16[4,32,1024]{2,1,0:T(8,128)(2,1)S(1)}, u32[]{:S(2)}, u32[]{:S(2)}) %all-to-all-start) | async-done | bytes 262176 | tf_op jit(solution)/shard_map/all_to_all | solution.py:193
  12.7 1.7 %project.1 = (bf16[4,128,1024]{2,1,0:T(8,128)(2,1)S(1)}, bf16[2,128,128]{2,1,0:T(8,128)(2,1)S(1)}) custom-call(s32[1]{0:T(128)} %bitcast.1.sp_ref, bf16[128,1024]{1,0:T(8,128)(2,1)S(1)} %bitcast.9, bf16[1024,1280]{1,0:T(8,128)(2,1)S(1)} %pad_maximum_fusion.w_ref, f32[1,1280]{1,0:T(1,128)S(1)} %reshape.27.vec_ref, f32[2,256,128]{2,1,0:T(8,128)S(1)} %copy-done.2, ...), custom_call_target="tpu_custom_call" | custom-call | flops 335544320 | bytes 1048576 | tf_op jit(solution)/shard_map/project/pallas_call | solution.py:196
  14.4 38.3 %all-gather.2 = f16[32,128,128]{2,1,0:T(8,128)(2,1)S(1)} all-gather(f16[2,128,128]{2,1,0:T(8,128)(2,1)S(1)} %convert_element_type.6), channel_id=2, replica_groups={{0,36,64,100,128,164,192,228,256,292,320,356,384,420,448,484},{4,32,68,..., dimensions={0}, use_global_device_ids=true | all-gather | bytes 1114112 | tf_op jit(solution)/shard_map/all_gather | solution.py:208
  53.1 2.0 %collective-permute-start = (bf16[16,2,128,128]{3,2,1,0:T(8,128)(2,1)S(1)}, bf16[16,2,128,128]{3,2,1,0:T(8,128)(2,1)S(1)}, u32[]{:S(2)}, u32[]{:S(2)}) collective-permute-start(bf16[16,2,128,128]{3,2,1,0:T(8,128)(2,1)S(1)} %bitcast.10), channel_id=1, source_target_pairs={{0,4},{4,0},{1,5},{5,1},{2,6},{6,2},{3,7},{7,3},{8,12},{12,8},{9,1... | collective-permute-start | bytes 3145736 | tf_op jit(solution)/shard_map/ppermute | solution.py:210
  55.1 4.3 %all-to-all-start.1 = ((bf16[4,128,1024]{2,1,0:T(8,128)(2,1)}), bf16[4,128,1024]{2,1,0:T(8,128)(2,1)S(1)}, u32[]{:S(2)}, u32[]{:S(2)}) async-start(bf16[4,128,1024]{2,1,0:T(8,128)(2,1)} %copy-done.1), calls=%async_computation.1 | async-start | bytes 2097152 | tf_op jit(solution)/shard_map/all_to_all | solution.py:206
  59.4 15.7 %all-to-all-done.1.refs_1_ = bf16[4,128,1024]{2,1,0:T(8,128)(2,1)S(1)} async-done(((bf16[4,128,1024]{2,1,0:T(8,128)(2,1)}), bf16[4,128,1024]{2,1,0:T(8,128)(2,1)S(1)}, u32[]{:S(2)}, u32[]{:S(2)}) %all-to-all-start.1) | async-done | bytes 1048608 | tf_op jit(solution)/shard_map/all_to_all | solution.py:206
  75.1 1.9 %shard_map.101.refs_3_ = f32[136,1024]{1,0:T(8,128)S(1)} custom-call(s32[1]{0:T(128)} %bitcast.4.refs_0_, bf16[4,128,1024]{2,1,0:T(8,128)(2,1)S(1)} %all-to-all-done.1.refs_1_, bf16[16,2,128,128]{3,2,1,0:T(8,128)(2,1)S(1)} %bitcast.11), custom_call_target="tpu_custom_call" | custom-call | flops 1073741824 | bytes 1048576 | tf_op jit(solution)/shard_map/pallas_call | solution.py:48
  77.0 4.3 %shard_map.103 = bf16[136,1024]{1,0:T(8,128)(2,1)} custom-call(s32[1]{0:T(128)} %bitcast.5.refs_0_, bf16[4,128,1024]{2,1,0:T(8,128)(2,1)S(1)} %all-to-all-done.1.refs_1_, bf16[16,2,128,128]{3,2,1,0:T(8,128)(2,1)S(1)} %bitcast.12, bf16[16,2,128,128]{3,2,1,0:T(8,128)(2,1)S(1)} %collective-permute-done.refs_3_.refs_2_), custom_call_target="tpu_custom_call" | custom-call | flops 2147483648 | bytes 1048576 | tf_op jit(solution)/shard_map/pallas_call | solution.py:48
  81.3 2.5 %collective-permute-start.2 = (bf16[136,1024]{1,0:T(8,128)(2,1)}, bf16[136,1024]{1,0:T(8,128)(2,1)S(1)}, u32[]{:S(2)}, u32[]{:S(2)}) collective-permute-start(bf16[136,1024]{1,0:T(8,128)(2,1)} %shard_map.103), channel_id=1, source_target_pairs={{0,8},{8,16},{16,24},{24,0},{1,9},{9,17},{17,25},{25,1},{2,10},{10... | collective-permute-start | bytes 835592 | tf_op jit(solution)/shard_map/ppermute | solution.py:214
  83.8 4.3 %shard_map.104 = bf16[136,1024]{1,0:T(8,128)(2,1)} custom-call(s32[1]{0:T(128)} %bitcast.6.refs_0_, bf16[4,128,1024]{2,1,0:T(8,128)(2,1)S(1)} %all-to-all-done.1.refs_1_, bf16[16,2,128,128]{3,2,1,0:T(8,128)(2,1)S(1)} %bitcast.13, bf16[16,2,128,128]{3,2,1,0:T(8,128)(2,1)S(1)} %collective-permute-done.refs_3_.refs_2_), custom_call_target="tpu_custom_call" | custom-call | flops 2147483648 | bytes 1048576 | tf_op jit(solution)/shard_map/pallas_call | solution.py:48
  88.1 4.8 %collective-permute-start.3 = (bf16[136,1024]{1,0:T(8,128)(2,1)}, bf16[136,1024]{1,0:T(8,128)(2,1)S(1)}, u32[]{:S(2)}, u32[]{:S(2)}) collective-permute-start(bf16[136,1024]{1,0:T(8,128)(2,1)} %shard_map.104), channel_id=1, source_target_pairs={{0,24},{8,0},{16,8},{24,16},{1,25},{9,1},{17,9},{25,17},{2,26},{10... | collective-permute-start | bytes 835592 | tf_op jit(solution)/shard_map/ppermute | solution.py:214
  92.8 1.2 %copy-done.5 = bf16[16,2,128,128]{3,2,1,0:T(8,128)(2,1)S(1)} copy-done((bf16[16,2,128,128]{3,2,1,0:T(8,128)(2,1)S(1)}, bf16[16,2,128,128]{3,2,1,0:T(8,128)(2,1)}, u32[]{:S(2)}) %copy-start.5) | copy-done | bytes 1048600
  94.0 1.9 %shard_map.102 = bf16[136,1024]{1,0:T(8,128)(2,1)S(1)} custom-call(s32[1]{0:T(128)} %bitcast.4.refs_0_, bf16[4,128,1024]{2,1,0:T(8,128)(2,1)S(1)} %all-to-all-done.1.refs_1_, bf16[16,2,128,128]{3,2,1,0:T(8,128)(2,1)S(1)} %copy-done.5, f32[136,1024]{1,0:T(8,128)S(1)} %shard_map.101.refs_3_), custom_call_target="tpu_custom_call" | custom-call | flops 1073741824 | bytes 1048576 | tf_op jit(solution)/shard_map/pallas_call | solution.py:48
  95.9 1.9 %collective-permute-start.1 = (bf16[136,1024]{1,0:T(8,128)(2,1)S(1)}, bf16[136,1024]{1,0:T(8,128)(2,1)S(1)}, u32[]{:S(2)}, u32[]{:S(2)}) collective-permute-start(bf16[136,1024]{1,0:T(8,128)(2,1)S(1)} %shard_map.102), channel_id=1, source_target_pairs={{0,16},{8,24},{16,0},{24,8},{1,17},{9,25},{17,1},{25,9},{2,18},{10... | collective-permute-start | bytes 835592 | tf_op jit(solution)/shard_map/ppermute | solution.py:214
  97.9 1.2 %copy-done.6 = bf16[16,2,128,128]{3,2,1,0:T(8,128)(2,1)S(1)} copy-done((bf16[16,2,128,128]{3,2,1,0:T(8,128)(2,1)S(1)}, bf16[16,2,128,128]{3,2,1,0:T(8,128)(2,1)}, u32[]{:S(2)}) %copy-start.6) | copy-done | bytes 1048600
  99.1 3.6 %shard_map.100.own_ref = f32[136,1024]{1,0:T(8,128)S(1)} custom-call(s32[1]{0:T(128)} %bitcast.refs_0_, bf16[4,128,1024]{2,1,0:T(8,128)(2,1)S(1)} %all-to-all-done.1.refs_1_, bf16[16,2,128,128]{3,2,1,0:T(8,128)(2,1)S(1)} %bitcast.14, bf16[16,2,128,128]{3,2,1,0:T(8,128)(2,1)S(1)} %copy-done.6), custom_call_target="tpu_custom_call" | custom-call | flops 2147483648 | bytes 1048576 | tf_op jit(solution)/shard_map/pallas_call | solution.py:48
  102.7 1.3 %collective-permute-done.3.refs_2_ = bf16[136,1024]{1,0:T(8,128)(2,1)S(1)} collective-permute-done((bf16[136,1024]{1,0:T(8,128)(2,1)}, bf16[136,1024]{1,0:T(8,128)(2,1)S(1)}, u32[]{:S(2)}, u32[]{:S(2)}) %collective-permute-start.3) | collective-permute-done | bytes 278560 | tf_op jit(solution)/shard_map/ppermute | solution.py:214
  104.0 2.6 %collective-permute-done.1.refs_0_ = bf16[136,1024]{1,0:T(8,128)(2,1)S(1)} collective-permute-done((bf16[136,1024]{1,0:T(8,128)(2,1)S(1)}, bf16[136,1024]{1,0:T(8,128)(2,1)S(1)}, u32[]{:S(2)}, u32[]{:S(2)}) %collective-permute-start.1) | collective-permute-done | bytes 278560 | tf_op jit(solution)/shard_map/ppermute | solution.py:214
  107.2 9.1 %all_to_all.15.part_ref = bf16[4,32,1024]{2,1,0:T(8,128)(2,1)S(1)} all-to-all(bf16[4,32,1024]{2,1,0:T(8,128)(2,1)S(1)} %bitcast.8), channel_id=1, replica_groups=mesh['z'=16,'x'=4,'c'=2,'y'=4] {'y'}, dimensions={0} | all-to-all | bytes 524288 | tf_op jit(solution)/shard_map/all_to_all | solution.py:225
  116.2 0.7 shard_map.106
  (18 shorter events, 0.9 us)
Async XLA Ops:
  1.6 11.2 %all-to-all-start = ((bf16[4,32,1024]{2,1,0:T(8,128)(2,1)}), bf16[4,32,1024]{2,1,0:T(8,128)(2,1)S(1)}, u32[]{:S(2)}, u32[]{:S(2)}) async-start(bf16[4,32,1024]{2,1,0:T(8,128)(2,1)} %spread.1), calls=%async_computation | async-start | bytes 524288 | tf_op jit(solution)/shard_map/all_to_all | solution.py:193
  6.8 5.9 %copy-start.2 = (f32[2,256,128]{2,1,0:T(8,128)S(1)}, f32[2,256,128]{2,1,0:T(8,128)}, u32[]{:S(2)}) copy-start(f32[2,256,128]{2,1,0:T(8,128)} %constant.50.clone.rows_ref) | copy-start | bytes 786436
  6.8 5.9 %copy-start.3 = (f32[2,64,128]{2,1,0:T(8,128)S(1)}, f32[2,64,128]{2,1,0:T(8,128)}, u32[]{:S(2)}) copy-start(f32[2,64,128]{2,1,0:T(8,128)} %constant.51.clone.cols_ref) | copy-start | bytes 196612
  14.4 40.7 %copy-start.1 = (bf16[4,128,1024]{2,1,0:T(8,128)(2,1)}, bf16[4,128,1024]{2,1,0:T(8,128)(2,1)S(1)}, u32[]{:S(2)}) copy-start(bf16[4,128,1024]{2,1,0:T(8,128)(2,1)S(1)} %get-tuple-element.7) | copy-start | bytes 3145732
  53.1 23.9 %collective-permute-start = (bf16[16,2,128,128]{3,2,1,0:T(8,128)(2,1)S(1)}, bf16[16,2,128,128]{3,2,1,0:T(8,128)(2,1)S(1)}, u32[]{:S(2)}, u32[]{:S(2)}) collective-permute-start(bf16[16,2,128,128]{3,2,1,0:T(8,128)(2,1)S(1)} %bitcast.10), channel_id=1, source_target_pairs={{0,4},{4,0},{1,5},{5,1},{2,6},{6,2},{3,7},{7,3},{8,12},{12,8},{9,1... | collective-permute-start | bytes 3145736 | tf_op jit(solution)/shard_map/ppermute | solution.py:210
  55.1 20.0 %all-to-all-start.1 = ((bf16[4,128,1024]{2,1,0:T(8,128)(2,1)}), bf16[4,128,1024]{2,1,0:T(8,128)(2,1)S(1)}, u32[]{:S(2)}, u32[]{:S(2)}) async-start(bf16[4,128,1024]{2,1,0:T(8,128)(2,1)} %copy-done.1), calls=%async_computation.1 | async-start | bytes 2097152 | tf_op jit(solution)/shard_map/all_to_all | solution.py:206
  77.0 6.8 %copy-start.4 = (bf16[16,2,128,128]{3,2,1,0:T(8,128)(2,1)}, bf16[16,2,128,128]{3,2,1,0:T(8,128)(2,1)S(1)}, u32[]{:S(2)}) copy-start(bf16[16,2,128,128]{3,2,1,0:T(8,128)(2,1)S(1)} %collective-permute-done.refs_3_.refs_2_) | copy-start | bytes 3145732
  81.3 21.4 %collective-permute-start.2 = (bf16[136,1024]{1,0:T(8,128)(2,1)}, bf16[136,1024]{1,0:T(8,128)(2,1)S(1)}, u32[]{:S(2)}, u32[]{:S(2)}) collective-permute-start(bf16[136,1024]{1,0:T(8,128)(2,1)} %shard_map.103), channel_id=1, source_target_pairs={{0,8},{8,16},{16,24},{24,0},{1,9},{9,17},{17,25},{25,1},{2,10},{10... | collective-permute-start | bytes 835592 | tf_op jit(solution)/shard_map/ppermute | solution.py:214
  88.1 16.0 %collective-permute-start.3 = (bf16[136,1024]{1,0:T(8,128)(2,1)}, bf16[136,1024]{1,0:T(8,128)(2,1)S(1)}, u32[]{:S(2)}, u32[]{:S(2)}) collective-permute-start(bf16[136,1024]{1,0:T(8,128)(2,1)} %shard_map.104), channel_id=1, source_target_pairs={{0,24},{8,0},{16,8},{24,16},{1,25},{9,1},{17,9},{25,17},{2,26},{10... | collective-permute-start | bytes 835592 | tf_op jit(solution)/shard_map/ppermute | solution.py:214
  92.8 1.2 %copy-start.5 = (bf16[16,2,128,128]{3,2,1,0:T(8,128)(2,1)S(1)}, bf16[16,2,128,128]{3,2,1,0:T(8,128)(2,1)}, u32[]{:S(2)}) copy-start(bf16[16,2,128,128]{3,2,1,0:T(8,128)(2,1)} %copy-done.4) | copy-start | bytes 3145732
  95.9 10.7 %collective-permute-start.1 = (bf16[136,1024]{1,0:T(8,128)(2,1)S(1)}, bf16[136,1024]{1,0:T(8,128)(2,1)S(1)}, u32[]{:S(2)}, u32[]{:S(2)}) collective-permute-start(bf16[136,1024]{1,0:T(8,128)(2,1)S(1)} %shard_map.102), channel_id=1, source_target_pairs={{0,16},{8,24},{16,0},{24,8},{1,17},{9,25},{17,1},{25,9},{2,18},{10... | collective-permute-start | bytes 835592 | tf_op jit(solution)/shard_map/ppermute | solution.py:214
  97.9 1.2 %copy-start.6 = (bf16[16,2,128,128]{3,2,1,0:T(8,128)(2,1)S(1)}, bf16[16,2,128,128]{3,2,1,0:T(8,128)(2,1)}, u32[]{:S(2)}) copy-start(bf16[16,2,128,128]{3,2,1,0:T(8,128)(2,1)} %copy-done.4) | copy-start | bytes 3145732
  99.1 7.5 %copy-start = (bf16[1024,1024]{1,0:T(8,128)(2,1)S(1)}, bf16[1024,1024]{1,0:T(8,128)(2,1)}, u32[]{:S(2)}) copy-start(bf16[1024,1024]{1,0:T(8,128)(2,1)} %refs_3_.1) | copy-start | bytes 6291460

commit v2 on v1

--- a/solution.py
+++ b/solution.py
@@ -134,7 +134,9 @@
     return jnp.concatenate([wide[:HD], wide[HD : HD + 1] + wide[HD + 1 : HD + 2]], axis=0)
 
 
-def fold_kernel(tiles, sets, resumed, packed, at_ref, q_ref, *refs):
+def fold_kernel(steps, sets, resumed, packed, sp_ref, q_ref, *refs):
+    tiles = len(steps)
+    x = (sp_ref[0] // NC) % NX
     kv_refs, sum_refs, out_refs = refs[:sets], refs[sets : len(refs) - tiles], refs[len(refs) - tiles :]
     ones = jnp.full((LROWS, CHUNK), VALUE_SCALE, jnp.bfloat16)
     per = CHUNK // TOK
@@ -145,7 +147,7 @@
             columns = jnp.concatenate([kv_ref[i, 1] for i in range(j, j + per)], axis=1)
             values.append(jnp.concatenate([columns, ones], axis=0))
     for t in range(tiles):
-        q = q_ref[at_ref[t]]
+        q = q_ref[(x + steps[t]) % NX]
         total = sum_refs[t][...] if resumed else None
         for k, v in zip(keys, values):
             weights = jnp.exp2(jnp.dot(k, q, preferred_element_type=jnp.float32)).astype(jnp.bfloat16)
@@ -154,16 +156,16 @@
         out_refs[t][...] = pack(total) if packed else total
 
 
-def fold(at, queries, blocks, sums=(), packed=False):
-    tiles = at.shape[0]
+def fold(sp, steps, queries, blocks, sums=(), packed=False):
+    tiles = len(steps)
     width = queries.shape[2]
     shape = tuple(bf16(PROWS, width) if packed else f32(AROWS, width) for _ in range(tiles))
 
     def kernel(*refs):
-        fold_kernel(tiles, len(blocks), len(sums) > 0, packed, *refs)
+        fold_kernel(steps, len(blocks), len(sums) > 0, packed, *refs)
 
     flops = 4 * tiles * width * sum(b.shape[0] for b in blocks) * TOK * HD
-    return call(kernel, shape, at, queries, *blocks, *sums, smem=1, flops=flops)
+    return call(kernel, shape, sp, queries, *blocks, *sums, smem=1, flops=flops)
 
 
 def finish_kernel(own_ref, *refs):
@@ -186,7 +188,7 @@
 
 def per_device(tables, tokens, norm_gain, wq, wk, wv, query_gain, key_gain, wo):
     z, x, c = (lax.axis_index(a) for a in ("z", "x", "c"))
-    sp = (z * NX + x) * NC + c
+    sp = jnp.reshape((z * NX + x) * NC + c, (1,)).astype(jnp.int32)
     rows, dim = tokens.shape
     width = wq.shape[1]
     copies = spread(tokens, NY)
@@ -202,25 +204,24 @@
         name="project",
         cost_estimate=pl.CostEstimate(flops=2 * TOK * dim * (width + 2 * HD), bytes_accessed=1 << 20, transcendentals=0),
         compiler_params=pltpu.CompilerParams(vmem_limit_bytes=24 << 20),
-    )(jnp.reshape(sp, (1,)).astype(jnp.int32), mine, weights, gains, *tables)
+    )(sp, mine, weights, gains, *tables)
     own_q = lax.all_to_all(q, "x", 0, 0, tiled=True)
     scaled = kv.astype(jnp.float16)
     gathered = lax.all_gather(scaled[None], ("z", "c"), axis_index_groups=RINGS, axis=0, tiled=True)
     blocks = gathered.astype(jnp.bfloat16)
     others = lax.ppermute(blocks, "c", [(0, 1), (1, 0)])
-    at = [jnp.reshape((x + d) % NX, (1,)).astype(jnp.int32) for d in range(NX)]
 
     def send(block, d):
         return lax.ppermute(block, "x", [(i, (i + d) % NX) for i in range(NX)])
 
-    (two,) = fold(at[2], own_q, (blocks,))
-    (two,) = fold(at[2], own_q, (others,), (two,), packed=True)
+    (two,) = fold(sp, (2,), own_q, (blocks,))
+    (two,) = fold(sp, (2,), own_q, (others,), (two,), packed=True)
     two = send(two, 2)
-    (one,) = fold(at[1], own_q, (blocks, others), packed=True)
+    (one,) = fold(sp, (1,), own_q, (blocks, others), packed=True)
     one = send(one, 1)
-    (three,) = fold(at[3], own_q, (blocks, others), packed=True)
+    (three,) = fold(sp, (3,), own_q, (blocks, others), packed=True)
     three = send(three, 3)
-    (kept,) = fold(at[0], own_q, (blocks, others))
+    (kept,) = fold(sp, (0,), own_q, (blocks, others))
     mixed = call(finish_kernel, bf16(TOK, wo.shape[1]), kept, two, one, three, wo, flops=2 * TOK * 1024 * 1024)
     shares = lax.all_to_all(mixed.reshape(NY, rows, -1), "y", 0, 0, tiled=True)
     return call(sum_kernel, bf16(rows, dim), shares)

time: 117 us -> 115 us (0.983)
  blocking collectives: 47.4 us -> 67.2 us
  waiting for transfers between devices: 23.4 us -> 9 us
  starting transfers between devices: 19.9 us -> 15.8 us
  local copies, waits for them, and re-layouts: 2.47 us -> 0.02 us
  Pallas kernels: 20.4 us -> 19 us
    all_to_all x0 -> x1, blocking collectives: none -> 19.8 us  [per_device(): own_q = lax.all_to_all(q, 'x', 0, 0, tiled=True)]
    all_to_all x1 -> x0, waiting for transfers between devices: 15.7 us -> none  [per_device(): own_q = lax.all_to_all(q, 'x', 0, 0, tiled=True)]
    all_to_all x1 -> x0, starting transfers between devices: 4.31 us -> none  [per_device(): own_q = lax.all_to_all(q, 'x', 0, 0, tiled=True)]
    unnamed x14 -> x6, local copies, waits for them, and re-layouts: 2.46 us -> 0.02 us
    pallas_call x7, Pallas kernels: 17.2 us -> 15.7 us  [call(): pl.pallas_call(kernel, out_shape=shapes, in_specs=[pl.BlockSpec(memory_sp...]
    ppermute x3, waiting for transfers between devices: 3.87 us -> 5.14 us  [send(): return lax.ppermute(block, 'x', [(i, (i + d) % NX) for i in range(NX)])]
  transfers between devices with their start and end apart: 6 -> 5, of which waited for: 4 -> 3; matrix products, arithmetic and copies ran while one was open for 2% -> 2% of each run, Pallas kernels for 10% -> 10%
where the time goes in v2:
time: 115 us; the launch traced here: 114 us
  blocking collectives  67.2 us (58%)
  Pallas kernels  19 us (17%)
  starting transfers between devices  15.8 us (14%)
  waiting for transfers between devices  9 us (8%)
  other arithmetic  3.1 us (3%)
    all_gather x1, blocking collectives, per_device(): lax.all_gather(scaled[None], ('z', 'c'), axis_index_groups=RINGS, axis=0,...  38.3 us
    all_to_all x1, blocking collectives, per_device(): own_q = lax.all_to_all(q, 'x', 0, 0, tiled=True)  19.8 us
    pallas_call x7, Pallas kernels, call(): pl.pallas_call(kernel, out_shape=shapes, in_specs=[pl.BlockSpec(memory_sp...  15.7 us
    ppermute x3, starting transfers between devices, send(): return lax.ppermute(block, 'x', [(i, (i + d) % NX) for i in range(NX)])  9.29 us
    all_to_all x1, blocking collectives, per_device(): shares = lax.all_to_all(mixed.reshape(NY, rows, -1), 'y', 0, 0, tiled=True)  9.07 us
    ppermute x3, waiting for transfers between devices, send(): return lax.ppermute(block, 'x', [(i, (i + d) % NX) for i in range(NX)])  5.14 us
    all_to_all x1, starting transfers between devices, per_device(): mine = lax.all_to_all(copies, 'y', 0, 0, tiled=True).reshape(NY * rows, dim)  4.48 us
    all_to_all x1, waiting for transfers between devices, per_device(): mine = lax.all_to_all(copies, 'y', 0, 0, tiled=True).reshape(NY * rows, dim)  3.85 us
  transfers between devices with their start and end apart: 5, of which 3 were waited for; matrix products, arithmetic and copies ran while one was open for 2% of the time, Pallas kernels for 10%

profile of v2, /device:TPU:32, one launch (start us, length us, event | category | flops | bytes accessed | tf_op | source)
XLA Modules:
  0.0 114.2 jit_solution(11390916562920570648)
XLA Ops:
  0.0 1.6 %spread.1 = bf16[4,32,1024]{2,1,0:T(8,128)(2,1)} custom-call(bf16[32,1024]{1,0:T(8,128)(2,1)} %tok_ref.1), custom_call_target="tpu_custom_call" | custom-call | tf_op jit(solution)/shard_map/spread/pallas_call | solution.py:76
  1.6 4.5 %all-to-all-start = ((bf16[4,32,1024]{2,1,0:T(8,128)(2,1)}), bf16[4,32,1024]{2,1,0:T(8,128)(2,1)S(1)}, u32[]{:S(2)}, u32[]{:S(2)}) async-start(bf16[4,32,1024]{2,1,0:T(8,128)(2,1)} %spread.1), calls=%async_computation | async-start | bytes 524288 | tf_op jit(solution)/shard_map/all_to_all | solution.py:195
  6.1 0.7 pad_maximum_fusion.1
  6.8 0.0 copy-start.2
  6.8 2.1 %pad_maximum_fusion.w_ref = bf16[1024,1280]{1,0:T(8,128)(2,1)S(1)} fusion(bf16[1024,128]{1,0:T(8,128)(2,1)} %param.14, bf16[1024,128]{1,0:T(8,128)(2,1)} %param.13, bf16[1024,1024]{1,0:T(8,128)(2,1)} %param.12), kind=kLoop, calls=%fused_computation | loop fusion | flops 7864320 | bytes 5242880 | tf_op jit(solution)/shard_map/concatenate | solution.py:196
  8.9 3.9 %all-to-all-done = bf16[4,32,1024]{2,1,0:T(8,128)(2,1)S(1)} async-done(((bf16[4,32,1024]{2,1,0:T(8,128)(2,1)}), bf16[4,32,1024]{2,1,0:T(8,128)(2,1)S(1)}, u32[]{:S(2)}, u32[]{:S(2)}) %all-to-all-start) | async-done | bytes 262176 | tf_op jit(solution)/shard_map/all_to_all | solution.py:195
  12.7 1.7 %project.1 = (bf16[4,128,1024]{2,1,0:T(8,128)(2,1)S(1)}, bf16[2,128,128]{2,1,0:T(8,128)(2,1)S(1)}) custom-call(s32[1]{0:T(128)} %bitcast.sp_ref.refs_0_, bf16[128,1024]{1,0:T(8,128)(2,1)S(1)} %bitcast.5, bf16[1024,1280]{1,0:T(8,128)(2,1)S(1)} %pad_maximum_fusion.w_ref, f32[1,1280]{1,0:T(1,128)S(1)} %reshape.14.vec_ref, f32[2,256,128]{2,1,0:T(8,128)S(1)} %copy-done.1, ...), custom_call_target="tpu_custom_call" | custom-call | flops 335544320 | bytes 1048576 | tf_op jit(solution)/shard_map/project/pallas_call | solution.py:198
  14.4 38.3 %all-gather.2 = f16[32,128,128]{2,1,0:T(8,128)(2,1)S(1)} all-gather(f16[2,128,128]{2,1,0:T(8,128)(2,1)S(1)} %convert_element_type.6), channel_id=2, replica_groups={{0,36,64,100,128,164,192,228,256,292,320,356,384,420,448,484},{4,32,68,..., dimensions={0}, use_global_device_ids=true | all-gather | bytes 1114112 | tf_op jit(solution)/shard_map/all_gather | solution.py:210
  52.8 0.3 convert_element_type.8
  53.1 2.0 %collective-permute-start = (bf16[16,2,128,128]{3,2,1,0:T(8,128)(2,1)S(1)}, bf16[16,2,128,128]{3,2,1,0:T(8,128)(2,1)S(1)}, u32[]{:S(2)}, u32[]{:S(2)}) collective-permute-start(bf16[16,2,128,128]{3,2,1,0:T(8,128)(2,1)S(1)} %bitcast.6), channel_id=1, source_target_pairs={{0,4},{4,0},{1,5},{5,1},{2,6},{6,2},{3,7},{7,3},{8,12},{12,8},{9,1... | collective-permute-start | bytes 3145736 | tf_op jit(solution)/shard_map/ppermute | solution.py:212
  55.1 19.8 %all_to_all.15.refs_1_ = bf16[4,128,1024]{2,1,0:T(8,128)(2,1)S(1)} all-to-all(bf16[4,128,1024]{2,1,0:T(8,128)(2,1)S(1)} %get-tuple-element.7), channel_id=1, replica_groups=mesh['z'=16,'x'=4,'c'=2,'y'=4] {'x'}, dimensions={0} | all-to-all | bytes 2097152 | tf_op jit(solution)/shard_map/all_to_all | solution.py:208
  74.9 1.9 %shard_map.101.refs_3_ = f32[136,1024]{1,0:T(8,128)S(1)} custom-call(s32[1]{0:T(128)} %bitcast.sp_ref.refs_0_, bf16[4,128,1024]{2,1,0:T(8,128)(2,1)S(1)} %all_to_all.15.refs_1_, bf16[16,2,128,128]{3,2,1,0:T(8,128)(2,1)S(1)} %bitcast.7), custom_call_target="tpu_custom_call" | custom-call | flops 1073741824 | bytes 1048576 | tf_op jit(solution)/shard_map/pallas_call | solution.py:48
  76.7 3.6 %shard_map.103 = bf16[136,1024]{1,0:T(8,128)(2,1)S(1)} custom-call(s32[1]{0:T(128)} %bitcast.sp_ref.refs_0_, bf16[4,128,1024]{2,1,0:T(8,128)(2,1)S(1)} %all_to_all.15.refs_1_, bf16[16,2,128,128]{3,2,1,0:T(8,128)(2,1)S(1)} %bitcast.8, bf16[16,2,128,128]{3,2,1,0:T(8,128)(2,1)S(1)} %collective-permute-done.refs_3_.refs_2_), custom_call_target="tpu_custom_call" | custom-call | flops 2147483648 | bytes 1048576 | tf_op jit(solution)/shard_map/pallas_call | solution.py:48
  80.4 2.5 %collective-permute-start.2 = (bf16[136,1024]{1,0:T(8,128)(2,1)S(1)}, bf16[136,1024]{1,0:T(8,128)(2,1)S(1)}, u32[]{:S(2)}, u32[]{:S(2)}) collective-permute-start(bf16[136,1024]{1,0:T(8,128)(2,1)S(1)} %shard_map.103), channel_id=1, source_target_pairs={{0,8},{8,16},{16,24},{24,0},{1,9},{9,17},{17,25},{25,1},{2,10},{10... | collective-permute-start | bytes 835592 | tf_op jit(solution)/shard_map/ppermute | solution.py:215
  82.8 3.6 %shard_map.104 = bf16[136,1024]{1,0:T(8,128)(2,1)S(1)} custom-call(s32[1]{0:T(128)} %bitcast.sp_ref.refs_0_, bf16[4,128,1024]{2,1,0:T(8,128)(2,1)S(1)} %all_to_all.15.refs_1_, bf16[16,2,128,128]{3,2,1,0:T(8,128)(2,1)S(1)} %bitcast.9, bf16[16,2,128,128]{3,2,1,0:T(8,128)(2,1)S(1)} %collective-permute-done.refs_3_.refs_2_), custom_call_target="tpu_custom_call" | custom-call | flops 2147483648 | bytes 1048576 | tf_op jit(solution)/shard_map/pallas_call | solution.py:48
  86.4 4.8 %collective-permute-start.3 = (bf16[136,1024]{1,0:T(8,128)(2,1)S(1)}, bf16[136,1024]{1,0:T(8,128)(2,1)S(1)}, u32[]{:S(2)}, u32[]{:S(2)}) collective-permute-start(bf16[136,1024]{1,0:T(8,128)(2,1)S(1)} %shard_map.104), channel_id=1, source_target_pairs={{0,24},{8,0},{16,8},{24,16},{1,25},{9,1},{17,9},{25,17},{2,26},{10... | collective-permute-start | bytes 835592 | tf_op jit(solution)/shard_map/ppermute | solution.py:215
  91.2 1.9 %shard_map.102 = bf16[136,1024]{1,0:T(8,128)(2,1)S(1)} custom-call(s32[1]{0:T(128)} %bitcast.sp_ref.refs_0_, bf16[4,128,1024]{2,1,0:T(8,128)(2,1)S(1)} %all_to_all.15.refs_1_, bf16[16,2,128,128]{3,2,1,0:T(8,128)(2,1)S(1)} %collective-permute-done.refs_3_.refs_2_, f32[136,1024]{1,0:T(8,128)S(1)} %shard_map.101.refs_3_), custom_call_target="tpu_custom_call" | custom-call | flops 1073741824 | bytes 1048576 | tf_op jit(solution)/shard_map/pallas_call | solution.py:48
  93.1 2.1 %collective-permute-start.1 = (bf16[136,1024]{1,0:T(8,128)(2,1)S(1)}, bf16[136,1024]{1,0:T(8,128)(2,1)S(1)}, u32[]{:S(2)}, u32[]{:S(2)}) collective-permute-start(bf16[136,1024]{1,0:T(8,128)(2,1)S(1)} %shard_map.102), channel_id=1, source_target_pairs={{0,16},{8,24},{16,0},{24,8},{1,17},{9,25},{17,1},{25,9},{2,18},{10... | collective-permute-start | bytes 835592 | tf_op jit(solution)/shard_map/ppermute | solution.py:215
  95.2 3.6 %shard_map.100.own_ref = f32[136,1024]{1,0:T(8,128)S(1)} custom-call(s32[1]{0:T(128)} %bitcast.sp_ref.refs_0_, bf16[4,128,1024]{2,1,0:T(8,128)(2,1)S(1)} %all_to_all.15.refs_1_, bf16[16,2,128,128]{3,2,1,0:T(8,128)(2,1)S(1)} %bitcast.10, bf16[16,2,128,128]{3,2,1,0:T(8,128)(2,1)S(1)} %collective-permute-done.refs_3_.refs_2_), custom_call_target="tpu_custom_call" | custom-call | flops 2147483648 | bytes 1048576 | tf_op jit(solution)/shard_map/pallas_call | solution.py:48
  98.8 3.3 %collective-permute-done.3.refs_2_ = bf16[136,1024]{1,0:T(8,128)(2,1)S(1)} collective-permute-done((bf16[136,1024]{1,0:T(8,128)(2,1)S(1)}, bf16[136,1024]{1,0:T(8,128)(2,1)S(1)}, u32[]{:S(2)}, u32[]{:S(2)}) %collective-permute-start.3) | collective-permute-done | bytes 278560 | tf_op jit(solution)/shard_map/ppermute | solution.py:215
  102.1 1.8 %collective-permute-done.1.refs_0_ = bf16[136,1024]{1,0:T(8,128)(2,1)S(1)} collective-permute-done((bf16[136,1024]{1,0:T(8,128)(2,1)S(1)}, bf16[136,1024]{1,0:T(8,128)(2,1)S(1)}, u32[]{:S(2)}, u32[]{:S(2)}) %collective-permute-start.1) | collective-permute-done | bytes 278560 | tf_op jit(solution)/shard_map/ppermute | solution.py:215
  104.0 0.5 shard_map.105
  104.5 9.1 %all_to_all.16.part_ref = bf16[4,32,1024]{2,1,0:T(8,128)(2,1)S(1)} all-to-all(bf16[4,32,1024]{2,1,0:T(8,128)(2,1)S(1)} %bitcast.4), channel_id=1, replica_groups=mesh['z'=16,'x'=4,'c'=2,'y'=4] {'y'}, dimensions={0} | all-to-all | bytes 524288 | tf_op jit(solution)/shard_map/all_to_all | solution.py:226
  113.6 0.7 shard_map.106
  (9 shorter events, 0.0 us)
Async XLA Ops:
  1.6 11.2 %all-to-all-start = ((bf16[4,32,1024]{2,1,0:T(8,128)(2,1)}), bf16[4,32,1024]{2,1,0:T(8,128)(2,1)S(1)}, u32[]{:S(2)}, u32[]{:S(2)}) async-start(bf16[4,32,1024]{2,1,0:T(8,128)(2,1)} %spread.1), calls=%async_computation | async-start | bytes 524288 | tf_op jit(solution)/shard_map/all_to_all | solution.py:195
  6.8 5.9 %copy-start.1 = (f32[2,256,128]{2,1,0:T(8,128)S(1)}, f32[2,256,128]{2,1,0:T(8,128)}, u32[]{:S(2)}) copy-start(f32[2,256,128]{2,1,0:T(8,128)} %constant.24.clone.rows_ref) | copy-start | bytes 786436
  6.8 5.9 %copy-start.2 = (f32[2,64,128]{2,1,0:T(8,128)S(1)}, f32[2,64,128]{2,1,0:T(8,128)}, u32[]{:S(2)}) copy-start(f32[2,64,128]{2,1,0:T(8,128)} %constant.25.clone.cols_ref) | copy-start | bytes 196612
  53.1 23.6 %collective-permute-start = (bf16[16,2,128,128]{3,2,1,0:T(8,128)(2,1)S(1)}, bf16[16,2,128,128]{3,2,1,0:T(8,128)(2,1)S(1)}, u32[]{:S(2)}, u32[]{:S(2)}) collective-permute-start(bf16[16,2,128,128]{3,2,1,0:T(8,128)(2,1)S(1)} %bitcast.6), channel_id=1, source_target_pairs={{0,4},{4,0},{1,5},{5,1},{2,6},{6,2},{3,7},{7,3},{8,12},{12,8},{9,1... | collective-permute-start | bytes 3145736 | tf_op jit(solution)/shard_map/ppermute | solution.py:212
  80.4 18.4 %collective-permute-start.2 = (bf16[136,1024]{1,0:T(8,128)(2,1)S(1)}, bf16[136,1024]{1,0:T(8,128)(2,1)S(1)}, u32[]{:S(2)}, u32[]{:S(2)}) collective-permute-start(bf16[136,1024]{1,0:T(8,128)(2,1)S(1)} %shard_map.103), channel_id=1, source_target_pairs={{0,8},{8,16},{16,24},{24,0},{1,9},{9,17},{17,25},{25,1},{2,10},{10... | collective-permute-start | bytes 835592 | tf_op jit(solution)/shard_map/ppermute | solution.py:215
  86.4 15.7 %collective-permute-start.3 = (bf16[136,1024]{1,0:T(8,128)(2,1)S(1)}, bf16[136,1024]{1,0:T(8,128)(2,1)S(1)}, u32[]{:S(2)}, u32[]{:S(2)}) collective-permute-start(bf16[136,1024]{1,0:T(8,128)(2,1)S(1)} %shard_map.104), channel_id=1, source_target_pairs={{0,24},{8,0},{16,8},{24,16},{1,25},{9,1},{17,9},{25,17},{2,26},{10... | collective-permute-start | bytes 835592 | tf_op jit(solution)/shard_map/ppermute | solution.py:215
  93.1 10.8 %copy-start = (bf16[1024,1024]{1,0:T(8,128)(2,1)S(1)}, bf16[1024,1024]{1,0:T(8,128)(2,1)}, u32[]{:S(2)}) copy-start(bf16[1024,1024]{1,0:T(8,128)(2,1)} %refs_3_.1) | copy-start | bytes 6291460
  93.1 10.8 %collective-permute-start.1 = (bf16[136,1024]{1,0:T(8,128)(2,1)S(1)}, bf16[136,1024]{1,0:T(8,128)(2,1)S(1)}, u32[]{:S(2)}, u32[]{:S(2)}) collective-permute-start(bf16[136,1024]{1,0:T(8,128)(2,1)S(1)} %shard_map.102), channel_id=1, source_target_pairs={{0,16},{8,24},{16,0},{24,8},{1,17},{9,25},{17,1},{25,9},{2,18},{10... | collective-permute-start | bytes 835592 | tf_op jit(solution)/shard_map/ppermute | solution.py:215

commit v3 on v2

--- a/solution.py
+++ b/solution.py
@@ -19,6 +19,7 @@
 LROWS = 8
 AROWS = HD + LROWS
 PROWS = HD + LROWS
+TURNS = ((1, 3), (2, 2), (3, 1))
 RINGS = [[i * NC + (i + g) % NC for i in range(NZ)] for g in range(NC)]
 CHUNK = 512
 
@@ -135,9 +136,8 @@
 
 
 def fold_kernel(steps, sets, resumed, packed, sp_ref, q_ref, *refs):
-    tiles = len(steps)
-    x = (sp_ref[0] // NC) % NX
-    kv_refs, sum_refs, out_refs = refs[:sets], refs[sets : len(refs) - tiles], refs[len(refs) - tiles :]
+    place = (sp_ref[0] // NC + steps[0] + sp_ref[0] % NC * (steps[1] - steps[0])) % NX
+    kv_refs, sum_ref, out_ref = refs[:sets], refs[sets], refs[-1]
     ones = jnp.full((LROWS, CHUNK), VALUE_SCALE, jnp.bfloat16)
     per = CHUNK // TOK
     keys, values = [], []
@@ -146,25 +146,23 @@
             keys.append(jnp.concatenate([kv_ref[i, 0] for i in range(j, j + per)], axis=0))
             columns = jnp.concatenate([kv_ref[i, 1] for i in range(j, j + per)], axis=1)
             values.append(jnp.concatenate([columns, ones], axis=0))
-    for t in range(tiles):
-        q = q_ref[(x + steps[t]) % NX]
-        total = sum_refs[t][...] if resumed else None
-        for k, v in zip(keys, values):
-            weights = jnp.exp2(jnp.dot(k, q, preferred_element_type=jnp.float32)).astype(jnp.bfloat16)
-            part = jnp.dot(v, weights, preferred_element_type=jnp.float32)
-            total = part if total is None else total + part
-        out_refs[t][...] = pack(total) if packed else total
+    q = q_ref[place]
+    total = sum_ref[...] if resumed else None
+    for k, v in zip(keys, values):
+        weights = jnp.exp2(jnp.dot(k, q, preferred_element_type=jnp.float32)).astype(jnp.bfloat16)
+        part = jnp.dot(v, weights, preferred_element_type=jnp.float32)
+        total = part if total is None else total + part
+    out_ref[...] = pack(total) if packed else total
 
 
 def fold(sp, steps, queries, blocks, sums=(), packed=False):
-    tiles = len(steps)
     width = queries.shape[2]
-    shape = tuple(bf16(PROWS, width) if packed else f32(AROWS, width) for _ in range(tiles))
+    shape = bf16(PROWS, width) if packed else f32(AROWS, width)
 
     def kernel(*refs):
         fold_kernel(steps, len(blocks), len(sums) > 0, packed, *refs)
 
-    flops = 4 * tiles * width * sum(b.shape[0] for b in blocks) * TOK * HD
+    flops = 4 * width * sum(b.shape[0] for b in blocks) * TOK * HD
     return call(kernel, shape, sp, queries, *blocks, *sums, smem=1, flops=flops)
 
 
@@ -211,18 +209,18 @@
     blocks = gathered.astype(jnp.bfloat16)
     others = lax.ppermute(blocks, "c", [(0, 1), (1, 0)])
 
-    def send(block, d):
-        return lax.ppermute(block, "x", [(i, (i + d) % NX) for i in range(NX)])
-
-    (two,) = fold(sp, (2,), own_q, (blocks,))
-    (two,) = fold(sp, (2,), own_q, (others,), (two,), packed=True)
-    two = send(two, 2)
-    (one,) = fold(sp, (1,), own_q, (blocks, others), packed=True)
-    one = send(one, 1)
-    (three,) = fold(sp, (3,), own_q, (blocks, others), packed=True)
-    three = send(three, 3)
-    (kept,) = fold(sp, (0,), own_q, (blocks, others))
-    mixed = call(finish_kernel, bf16(TOK, wo.shape[1]), kept, two, one, three, wo, flops=2 * TOK * 1024 * 1024)
+    def send(block, slot):
+        pairs = [(i * NC + j, (i + TURNS[slot][j]) % NX * NC + j) for i in range(NX) for j in range(NC)]
+        return lax.ppermute(block, ("x", "c"), pairs)
+
+    begun = fold(sp, TURNS[0], own_q, (blocks,))
+    sums = fold(sp, TURNS[0], own_q, (others,), (begun,), packed=True)
+    came = [send(sums, 0)]
+    for slot in (1, 2):
+        sums = fold(sp, TURNS[slot], own_q, (blocks, others), packed=True)
+        came.append(send(sums, slot))
+    kept = fold(sp, (0, 0), own_q, (blocks, others))
+    mixed = call(finish_kernel, bf16(TOK, wo.shape[1]), kept, *came, wo, flops=2 * TOK * 1024 * 1024)
     shares = lax.all_to_all(mixed.reshape(NY, rows, -1), "y", 0, 0, tiled=True)
     return call(sum_kernel, bf16(rows, dim), shares)
 

time: 115 us -> 114 us (level)
  transfers between devices with their start and end apart: 5 -> 5, of which waited for: 3 -> 2; matrix products, arithmetic and copies ran while one was open for 2% -> 2% of each run, Pallas kernels for 10% -> 10%
where the time goes in v3:
time: 114 us; the launch traced here: 113 us
  blocking collectives  67.2 us (59%)
  Pallas kernels  19 us (17%)
  starting transfers between devices  15.8 us (14%)
  waiting for transfers between devices  7.97 us (7%)
  other arithmetic  3.1 us (3%)
    all_gather x1, blocking collectives, per_device(): lax.all_gather(scaled[None], ('z', 'c'), axis_index_groups=RINGS, axis=0,...  38.3 us
    all_to_all x1, blocking collectives, per_device(): own_q = lax.all_to_all(q, 'x', 0, 0, tiled=True)  19.8 us
    pallas_call x7, Pallas kernels, call(): pl.pallas_call(kernel, out_shape=shapes, in_specs=[pl.BlockSpec(memory_sp...  15.7 us
    ppermute x3, starting transfers between devices, send(): return lax.ppermute(block, ('x', 'c'), pairs)  9.29 us
    all_to_all x1, blocking collectives, per_device(): shares = lax.all_to_all(mixed.reshape(NY, rows, -1), 'y', 0, 0, tiled=True)  9.07 us
    all_to_all x1, starting transfers between devices, per_device(): mine = lax.all_to_all(copies, 'y', 0, 0, tiled=True).reshape(NY * rows, dim)  4.48 us
    ppermute x3, waiting for transfers between devices, send(): return lax.ppermute(block, ('x', 'c'), pairs)  4.11 us
    all_to_all x1, waiting for transfers between devices, per_device(): mine = lax.all_to_all(copies, 'y', 0, 0, tiled=True).reshape(NY * rows, dim)  3.85 us
  transfers between devices with their start and end apart: 5, of which 2 were waited for; matrix products, arithmetic and copies ran while one was open for 2% of the time, Pallas kernels for 10%

profile of v3, /device:TPU:32, one launch (start us, length us, event | category | flops | bytes accessed | tf_op | source)
XLA Modules:
  0.0 113.2 jit_solution(9224565079748670367)
XLA Ops:
  0.0 1.6 %spread.1 = bf16[4,32,1024]{2,1,0:T(8,128)(2,1)} custom-call(bf16[32,1024]{1,0:T(8,128)(2,1)} %tok_ref.1), custom_call_target="tpu_custom_call" | custom-call | tf_op jit(solution)/shard_map/spread/pallas_call | solution.py:77
  1.6 4.5 %all-to-all-start = ((bf16[4,32,1024]{2,1,0:T(8,128)(2,1)}), bf16[4,32,1024]{2,1,0:T(8,128)(2,1)S(1)}, u32[]{:S(2)}, u32[]{:S(2)}) async-start(bf16[4,32,1024]{2,1,0:T(8,128)(2,1)} %spread.1), calls=%async_computation | async-start | bytes 524288 | tf_op jit(solution)/shard_map/all_to_all | solution.py:193
  6.1 0.7 pad_maximum_fusion.1
  6.8 0.0 copy-start.1
  6.8 0.0 copy-start.2
  6.8 2.1 %pad_maximum_fusion.w_ref = bf16[1024,1280]{1,0:T(8,128)(2,1)S(1)} fusion(bf16[1024,128]{1,0:T(8,128)(2,1)} %param.14, bf16[1024,128]{1,0:T(8,128)(2,1)} %param.13, bf16[1024,1024]{1,0:T(8,128)(2,1)} %param.12), kind=kLoop, calls=%fused_computation | loop fusion | flops 7864320 | bytes 5242880 | tf_op jit(solution)/shard_map/concatenate | solution.py:194
  8.9 3.9 %all-to-all-done = bf16[4,32,1024]{2,1,0:T(8,128)(2,1)S(1)} async-done(((bf16[4,32,1024]{2,1,0:T(8,128)(2,1)}), bf16[4,32,1024]{2,1,0:T(8,128)(2,1)S(1)}, u32[]{:S(2)}, u32[]{:S(2)}) %all-to-all-start) | async-done | bytes 262176 | tf_op jit(solution)/shard_map/all_to_all | solution.py:193
  12.7 1.7 %project.1 = (bf16[4,128,1024]{2,1,0:T(8,128)(2,1)S(1)}, bf16[2,128,128]{2,1,0:T(8,128)(2,1)S(1)}) custom-call(s32[1]{0:T(128)} %bitcast.sp_ref.refs_0_, bf16[128,1024]{1,0:T(8,128)(2,1)S(1)} %bitcast.5, bf16[1024,1280]{1,0:T(8,128)(2,1)S(1)} %pad_maximum_fusion.w_ref, f32[1,1280]{1,0:T(1,128)S(1)} %reshape.14.vec_ref, f32[2,256,128]{2,1,0:T(8,128)S(1)} %copy-done.1, ...), custom_call_target="tpu_custom_call" | custom-call | flops 335544320 | bytes 1048576 | tf_op jit(solution)/shard_map/project/pallas_call | solution.py:196
  14.4 38.3 %all-gather.2 = f16[32,128,128]{2,1,0:T(8,128)(2,1)S(1)} all-gather(f16[2,128,128]{2,1,0:T(8,128)(2,1)S(1)} %convert_element_type.6), channel_id=2, replica_groups={{0,36,64,100,128,164,192,228,256,292,320,356,384,420,448,484},{4,32,68,..., dimensions={0}, use_global_device_ids=true | all-gather | bytes 1114112 | tf_op jit(solution)/shard_map/all_gather | solution.py:208
  52.8 0.3 convert_element_type.8
  53.1 2.0 %collective-permute-start = (bf16[16,2,128,128]{3,2,1,0:T(8,128)(2,1)S(1)}, bf16[16,2,128,128]{3,2,1,0:T(8,128)(2,1)S(1)}, u32[]{:S(2)}, u32[]{:S(2)}) collective-permute-start(bf16[16,2,128,128]{3,2,1,0:T(8,128)(2,1)S(1)} %bitcast.6), channel_id=1, source_target_pairs={{0,4},{4,0},{1,5},{5,1},{2,6},{6,2},{3,7},{7,3},{8,12},{12,8},{9,1... | collective-permute-start | bytes 3145736 | tf_op jit(solution)/shard_map/ppermute | solution.py:210
  55.1 19.8 %all_to_all.15.refs_1_ = bf16[4,128,1024]{2,1,0:T(8,128)(2,1)S(1)} all-to-all(bf16[4,128,1024]{2,1,0:T(8,128)(2,1)S(1)} %get-tuple-element.7), channel_id=1, replica_groups=mesh['z'=16,'x'=4,'c'=2,'y'=4] {'x'}, dimensions={0} | all-to-all | bytes 2097152 | tf_op jit(solution)/shard_map/all_to_all | solution.py:206
  74.9 1.9 %shard_map.101.refs_3_ = f32[136,1024]{1,0:T(8,128)S(1)} custom-call(s32[1]{0:T(128)} %bitcast.sp_ref.refs_0_, bf16[4,128,1024]{2,1,0:T(8,128)(2,1)S(1)} %all_to_all.15.refs_1_, bf16[16,2,128,128]{3,2,1,0:T(8,128)(2,1)S(1)} %bitcast.7), custom_call_target="tpu_custom_call" | custom-call | flops 1073741824 | bytes 1048576 | tf_op jit(solution)/shard_map/pallas_call | solution.py:49
  76.7 3.6 %shard_map.103 = bf16[136,1024]{1,0:T(8,128)(2,1)S(1)} custom-call(s32[1]{0:T(128)} %bitcast.sp_ref.refs_0_, bf16[4,128,1024]{2,1,0:T(8,128)(2,1)S(1)} %all_to_all.15.refs_1_, bf16[16,2,128,128]{3,2,1,0:T(8,128)(2,1)S(1)} %bitcast.8, bf16[16,2,128,128]{3,2,1,0:T(8,128)(2,1)S(1)} %collective-permute-done.refs_3_.refs_2_), custom_call_target="tpu_custom_call" | custom-call | flops 2147483648 | bytes 1048576 | tf_op jit(solution)/shard_map/pallas_call | solution.py:49
  80.3 2.7 %collective-permute-start.2 = (bf16[136,1024]{1,0:T(8,128)(2,1)S(1)}, bf16[136,1024]{1,0:T(8,128)(2,1)S(1)}, u32[]{:S(2)}, u32[]{:S(2)}) collective-permute-start(bf16[136,1024]{1,0:T(8,128)(2,1)S(1)} %shard_map.103), channel_id=1, source_target_pairs={{0,16},{4,20},{8,24},{12,28},{16,0},{20,4},{24,8},{28,12},{1,17},{... | collective-permute-start | bytes 835592 | tf_op jit(solution)/shard_map/ppermute | solution.py:214
  83.1 3.6 %shard_map.104 = bf16[136,1024]{1,0:T(8,128)(2,1)S(1)} custom-call(s32[1]{0:T(128)} %bitcast.sp_ref.refs_0_, bf16[4,128,1024]{2,1,0:T(8,128)(2,1)S(1)} %all_to_all.15.refs_1_, bf16[16,2,128,128]{3,2,1,0:T(8,128)(2,1)S(1)} %bitcast.9, bf16[16,2,128,128]{3,2,1,0:T(8,128)(2,1)S(1)} %collective-permute-done.refs_3_.refs_2_), custom_call_target="tpu_custom_call" | custom-call | flops 2147483648 | bytes 1048576 | tf_op jit(solution)/shard_map/pallas_call | solution.py:49
  86.7 4.5 %collective-permute-start.3 = (bf16[136,1024]{1,0:T(8,128)(2,1)S(1)}, bf16[136,1024]{1,0:T(8,128)(2,1)S(1)}, u32[]{:S(2)}, u32[]{:S(2)}) collective-permute-start(bf16[136,1024]{1,0:T(8,128)(2,1)S(1)} %shard_map.104), channel_id=1, source_target_pairs={{0,24},{4,12},{8,0},{12,20},{16,8},{20,28},{24,16},{28,4},{1,25},{... | collective-permute-start | bytes 835592 | tf_op jit(solution)/shard_map/ppermute | solution.py:214
  91.2 1.9 %shard_map.102 = bf16[136,1024]{1,0:T(8,128)(2,1)S(1)} custom-call(s32[1]{0:T(128)} %bitcast.sp_ref.refs_0_, bf16[4,128,1024]{2,1,0:T(8,128)(2,1)S(1)} %all_to_all.15.refs_1_, bf16[16,2,128,128]{3,2,1,0:T(8,128)(2,1)S(1)} %collective-permute-done.refs_3_.refs_2_, f32[136,1024]{1,0:T(8,128)S(1)} %shard_map.101.refs_3_), custom_call_target="tpu_custom_call" | custom-call | flops 1073741824 | bytes 1048576 | tf_op jit(solution)/shard_map/pallas_call | solution.py:49
  93.1 2.1 %collective-permute-start.1 = (bf16[136,1024]{1,0:T(8,128)(2,1)S(1)}, bf16[136,1024]{1,0:T(8,128)(2,1)S(1)}, u32[]{:S(2)}, u32[]{:S(2)}) collective-permute-start(bf16[136,1024]{1,0:T(8,128)(2,1)S(1)} %shard_map.102), channel_id=1, source_target_pairs={{0,8},{4,28},{8,16},{12,4},{16,24},{20,12},{24,0},{28,20},{1,9},{5... | collective-permute-start | bytes 835592 | tf_op jit(solution)/shard_map/ppermute | solution.py:214
  95.2 3.6 %shard_map.100.own_ref = f32[136,1024]{1,0:T(8,128)S(1)} custom-call(s32[1]{0:T(128)} %bitcast.sp_ref.refs_0_, bf16[4,128,1024]{2,1,0:T(8,128)(2,1)S(1)} %all_to_all.15.refs_1_, bf16[16,2,128,128]{3,2,1,0:T(8,128)(2,1)S(1)} %bitcast.10, bf16[16,2,128,128]{3,2,1,0:T(8,128)(2,1)S(1)} %collective-permute-done.refs_3_.refs_2_), custom_call_target="tpu_custom_call" | custom-call | flops 2147483648 | bytes 1048576 | tf_op jit(solution)/shard_map/pallas_call | solution.py:49
  98.8 4.1 %collective-permute-done.1.refs_0_ = bf16[136,1024]{1,0:T(8,128)(2,1)S(1)} collective-permute-done((bf16[136,1024]{1,0:T(8,128)(2,1)S(1)}, bf16[136,1024]{1,0:T(8,128)(2,1)S(1)}, u32[]{:S(2)}, u32[]{:S(2)}) %collective-permute-start.1) | collective-permute-done | bytes 278560 | tf_op jit(solution)/shard_map/ppermute | solution.py:214
  102.9 0.5 shard_map.105
  103.4 9.1 %all_to_all.16.part_ref = bf16[4,32,1024]{2,1,0:T(8,128)(2,1)S(1)} all-to-all(bf16[4,32,1024]{2,1,0:T(8,128)(2,1)S(1)} %bitcast.4), channel_id=1, replica_groups=mesh['z'=16,'x'=4,'c'=2,'y'=4] {'y'}, dimensions={0} | all-to-all | bytes 524288 | tf_op jit(solution)/shard_map/all_to_all | solution.py:224
  112.5 0.7 shard_map.106
  (9 shorter events, 0.0 us)
Async XLA Ops:
  1.6 11.2 %all-to-all-start = ((bf16[4,32,1024]{2,1,0:T(8,128)(2,1)}), bf16[4,32,1024]{2,1,0:T(8,128)(2,1)S(1)}, u32[]{:S(2)}, u32[]{:S(2)}) async-start(bf16[4,32,1024]{2,1,0:T(8,128)(2,1)} %spread.1), calls=%async_computation | async-start | bytes 524288 | tf_op jit(solution)/shard_map/all_to_all | solution.py:193
  6.8 5.9 %copy-start.1 = (f32[2,256,128]{2,1,0:T(8,128)S(1)}, f32[2,256,128]{2,1,0:T(8,128)}, u32[]{:S(2)}) copy-start(f32[2,256,128]{2,1,0:T(8,128)} %constant.24.clone.rows_ref) | copy-start | bytes 786436
  6.8 5.9 %copy-start.2 = (f32[2,64,128]{2,1,0:T(8,128)S(1)}, f32[2,64,128]{2,1,0:T(8,128)}, u32[]{:S(2)}) copy-start(f32[2,64,128]{2,1,0:T(8,128)} %constant.25.clone.cols_ref) | copy-start | bytes 196612
  53.1 23.6 %collective-permute-start = (bf16[16,2,128,128]{3,2,1,0:T(8,128)(2,1)S(1)}, bf16[16,2,128,128]{3,2,1,0:T(8,128)(2,1)S(1)}, u32[]{:S(2)}, u32[]{:S(2)}) collective-permute-start(bf16[16,2,128,128]{3,2,1,0:T(8,128)(2,1)S(1)} %bitcast.6), channel_id=1, source_target_pairs={{0,4},{4,0},{1,5},{5,1},{2,6},{6,2},{3,7},{7,3},{8,12},{12,8},{9,1... | collective-permute-start | bytes 3145736 | tf_op jit(solution)/shard_map/ppermute | solution.py:210
  80.3 18.4 %collective-permute-start.2 = (bf16[136,1024]{1,0:T(8,128)(2,1)S(1)}, bf16[136,1024]{1,0:T(8,128)(2,1)S(1)}, u32[]{:S(2)}, u32[]{:S(2)}) collective-permute-start(bf16[136,1024]{1,0:T(8,128)(2,1)S(1)} %shard_map.103), channel_id=1, source_target_pairs={{0,16},{4,20},{8,24},{12,28},{16,0},{20,4},{24,8},{28,12},{1,17},{... | collective-permute-start | bytes 835592 | tf_op jit(solution)/shard_map/ppermute | solution.py:214
  86.7 12.1 %collective-permute-start.3 = (bf16[136,1024]{1,0:T(8,128)(2,1)S(1)}, bf16[136,1024]{1,0:T(8,128)(2,1)S(1)}, u32[]{:S(2)}, u32[]{:S(2)}) collective-permute-start(bf16[136,1024]{1,0:T(8,128)(2,1)S(1)} %shard_map.104), channel_id=1, source_target_pairs={{0,24},{4,12},{8,0},{12,20},{16,8},{20,28},{24,16},{28,4},{1,25},{... | collective-permute-start | bytes 835592 | tf_op jit(solution)/shard_map/ppermute | solution.py:214
  93.1 9.8 %copy-start = (bf16[1024,1024]{1,0:T(8,128)(2,1)S(1)}, bf16[1024,1024]{1,0:T(8,128)(2,1)}, u32[]{:S(2)}) copy-start(bf16[1024,1024]{1,0:T(8,128)(2,1)} %refs_3_.1) | copy-start | bytes 6291460
  93.1 9.8 %collective-permute-start.1 = (bf16[136,1024]{1,0:T(8,128)(2,1)S(1)}, bf16[136,1024]{1,0:T(8,128)(2,1)S(1)}, u32[]{:S(2)}, u32[]{:S(2)}) collective-permute-start(bf16[136,1024]{1,0:T(8,128)(2,1)S(1)} %shard_map.102), channel_id=1, source_target_pairs={{0,8},{4,28},{8,16},{12,4},{16,24},{20,12},{24,0},{28,20},{1,9},{5... | collective-permute-start | bytes 835592 | tf_op jit(solution)/shard_map/ppermute | solution.py:214

commit v4 on v3

--- a/solution.py
+++ b/solution.py
@@ -21,7 +21,7 @@
 PROWS = HD + LROWS
 TURNS = ((1, 3), (2, 2), (3, 1))
 RINGS = [[i * NC + (i + g) % NC for i in range(NZ)] for g in range(NC)]
-CHUNK = 512
+CHUNK = 1024
 
 
 def rotary_tables(grid_rows):
@@ -84,7 +84,7 @@
     )(array)
 
 
-def project_kernel(sp_ref, tok_ref, w_ref, vec_ref, rows_ref, cols_ref, q_ref, kv_ref, turned_ref, sems):
+def project_kernel(sp_ref, tok_ref, w_ref, vec_ref, rows_ref, cols_ref, q_ref, kv_ref):
     x = tok_ref[...].astype(jnp.float32)
     dim = x.shape[1]
     wide_q = w_ref.shape[1] - 2 * HD
@@ -115,12 +115,7 @@
     fold = HD ** (-0.5) * math.log2(math.e) / KEY_SCALE
     for h in range(queries.shape[1] // HD):
         turned = turn(queries[:, h * HD : (h + 1) * HD], query_gain) * fold
-        turned_ref[:, h * TOK : (h + 1) * TOK] = turned.T.astype(jnp.bfloat16)
-    copies = [pltpu.make_async_copy(turned_ref, q_ref.at[i], sems.at[i]) for i in range(NX)]
-    for copy in copies:
-        copy.start()
-    for copy in copies:
-        copy.wait()
+        q_ref[:, h * TOK : (h + 1) * TOK] = turned.T.astype(jnp.bfloat16)
 
 
 def pack(total):
@@ -195,15 +190,14 @@
     gains = jnp.concatenate([norm_gain, query_gain, key_gain]).reshape(1, -1)
     q, kv = pl.pallas_call(
         project_kernel,
-        out_shape=(bf16(NX, HD, width), bf16(2, TOK, HD)),
+        out_shape=(bf16(HD, width), bf16(2, TOK, HD)),
         in_specs=[pl.BlockSpec(memory_space=pltpu.SMEM)] + [VM] * 5,
-        out_specs=(pl.BlockSpec(memory_space=pltpu.HBM), VM),
-        scratch_shapes=[pltpu.VMEM((HD, width), jnp.bfloat16), pltpu.SemaphoreType.DMA((NX,))],
+        out_specs=(VM, VM),
         name="project",
         cost_estimate=pl.CostEstimate(flops=2 * TOK * dim * (width + 2 * HD), bytes_accessed=1 << 20, transcendentals=0),
         compiler_params=pltpu.CompilerParams(vmem_limit_bytes=24 << 20),
     )(sp, mine, weights, gains, *tables)
-    own_q = lax.all_to_all(q, "x", 0, 0, tiled=True)
+    own_q = lax.all_to_all(jnp.broadcast_to(q[None], (NX,) + q.shape), "x", 0, 0, tiled=True)
     scaled = kv.astype(jnp.float16)
     gathered = lax.all_gather(scaled[None], ("z", "c"), axis_index_groups=RINGS, axis=0, tiled=True)
     blocks = gathered.astype(jnp.bfloat16)

time: 114 us -> 114 us (level)
  transfers between devices with their start and end apart: 5 -> 5, of which waited for: 2 -> 2; matrix products, arithmetic and copies ran while one was open for 2% -> 3% of each run, Pallas kernels for 10% -> 10%
where the time goes in v4:
time: 114 us; the launch traced here: 113 us
  blocking collectives  67.2 us (59%)
  Pallas kernels  18.6 us (16%)
  starting transfers between devices  15.8 us (14%)
  waiting for transfers between devices  8.01 us (7%)
  other arithmetic  3.1 us (3%)
    all_gather x1, blocking collectives, per_device(): lax.all_gather(scaled[None], ('z', 'c'), axis_index_groups=RINGS, axis=0,...  38.3 us
    all_to_all x1, blocking collectives, per_device(): lax.all_to_all(jnp.broadcast_to(q[None], (NX,) + q.shape), 'x', 0, 0, til...  19.8 us
    pallas_call x7, Pallas kernels, call(): pl.pallas_call(kernel, out_shape=shapes, in_specs=[pl.BlockSpec(memory_sp...  15.5 us
    ppermute x3, starting transfers between devices, send(): return lax.ppermute(block, ('x', 'c'), pairs)  9.3 us
    all_to_all x1, blocking collectives, per_device(): shares = lax.all_to_all(mixed.reshape(NY, rows, -1), 'y', 0, 0, tiled=True)  9.07 us
    all_to_all x1, starting transfers between devices, per_device(): mine = lax.all_to_all(copies, 'y', 0, 0, tiled=True).reshape(NY * rows, dim)  4.48 us
    ppermute x3, waiting for transfers between devices, send(): return lax.ppermute(block, ('x', 'c'), pairs)  4.16 us
    all_to_all x1, waiting for transfers between devices, per_device(): mine = lax.all_to_all(copies, 'y', 0, 0, tiled=True).reshape(NY * rows, dim)  3.85 us
  transfers between devices with their start and end apart: 5, of which 2 were waited for; matrix products, arithmetic and copies ran while one was open for 3% of the time, Pallas kernels for 10%

profile of v4, /device:TPU:32, one launch (start us, length us, event | category | flops | bytes accessed | tf_op | source)
XLA Modules:
  0.0 113.0 jit_solution(10710146809173665030)
XLA Ops:
  0.0 1.6 %spread.1 = bf16[4,32,1024]{2,1,0:T(8,128)(2,1)} custom-call(bf16[32,1024]{1,0:T(8,128)(2,1)} %tok_ref.1), custom_call_target="tpu_custom_call" | custom-call | tf_op jit(solution)/shard_map/spread/pallas_call | solution.py:77
  1.6 4.5 %all-to-all-start = ((bf16[4,32,1024]{2,1,0:T(8,128)(2,1)}), bf16[4,32,1024]{2,1,0:T(8,128)(2,1)S(1)}, u32[]{:S(2)}, u32[]{:S(2)}) async-start(bf16[4,32,1024]{2,1,0:T(8,128)(2,1)} %spread.1), calls=%async_computation | async-start | bytes 524288 | tf_op jit(solution)/shard_map/all_to_all | solution.py:188
  6.1 0.7 pad_maximum_fusion.1
  6.8 0.0 copy-start.2
  6.8 2.1 %pad_maximum_fusion.w_ref = bf16[1024,1280]{1,0:T(8,128)(2,1)S(1)} fusion(bf16[1024,128]{1,0:T(8,128)(2,1)} %param.14, bf16[1024,128]{1,0:T(8,128)(2,1)} %param.13, bf16[1024,1024]{1,0:T(8,128)(2,1)} %param.12), kind=kLoop, calls=%fused_computation | loop fusion | flops 7864320 | bytes 5242880 | tf_op jit(solution)/shard_map/concatenate | solution.py:189
  8.9 3.9 %all-to-all-done = bf16[4,32,1024]{2,1,0:T(8,128)(2,1)S(1)} async-done(((bf16[4,32,1024]{2,1,0:T(8,128)(2,1)}), bf16[4,32,1024]{2,1,0:T(8,128)(2,1)S(1)}, u32[]{:S(2)}, u32[]{:S(2)}) %all-to-all-start) | async-done | bytes 262176 | tf_op jit(solution)/shard_map/all_to_all | solution.py:188
  12.7 1.6 %project.1 = (bf16[128,1024]{1,0:T(8,128)(2,1)S(1)}, bf16[2,128,128]{2,1,0:T(8,128)(2,1)S(1)}) custom-call(s32[1]{0:T(128)} %bitcast.sp_ref.refs_0_, bf16[128,1024]{1,0:T(8,128)(2,1)S(1)} %bitcast.5, bf16[1024,1280]{1,0:T(8,128)(2,1)S(1)} %pad_maximum_fusion.w_ref, f32[1,1280]{1,0:T(1,128)S(1)} %reshape.15.vec_ref, f32[2,256,128]{2,1,0:T(8,128)S(1)} %copy-done.1, ...), custom_call_target="tpu_custom_call" | custom-call | flops 335544320 | bytes 1048576 | tf_op jit(solution)/shard_map/project/pallas_call | solution.py:191
  14.3 38.3 %all-gather.2 = f16[32,128,128]{2,1,0:T(8,128)(2,1)S(1)} all-gather(f16[2,128,128]{2,1,0:T(8,128)(2,1)S(1)} %convert_element_type.6), channel_id=2, replica_groups={{0,36,64,100,128,164,192,228,256,292,320,356,384,420,448,484},{4,32,68,..., dimensions={0}, use_global_device_ids=true | all-gather | bytes 1114112 | tf_op jit(solution)/shard_map/all_gather | solution.py:202
  52.7 0.3 convert_element_type.8
  53.0 2.0 %collective-permute-start = (bf16[16,2,128,128]{3,2,1,0:T(8,128)(2,1)S(1)}, bf16[16,2,128,128]{3,2,1,0:T(8,128)(2,1)S(1)}, u32[]{:S(2)}, u32[]{:S(2)}) collective-permute-start(bf16[16,2,128,128]{3,2,1,0:T(8,128)(2,1)S(1)} %bitcast.6), channel_id=1, source_target_pairs={{0,4},{4,0},{1,5},{5,1},{2,6},{6,2},{3,7},{7,3},{8,12},{12,8},{9,1... | collective-permute-start | bytes 3145736 | tf_op jit(solution)/shard_map/ppermute | solution.py:204
  55.0 0.1 broadcast_in_dim.4
  55.1 19.8 %all_to_all.15.refs_1_ = bf16[4,128,1024]{2,1,0:T(8,128)(2,1)S(1)} all-to-all(bf16[4,128,1024]{2,1,0:T(8,128)(2,1)S(1)} %broadcast_in_dim.4), channel_id=1, replica_groups=mesh['z'=16,'x'=4,'c'=2,'y'=4] {'x'}, dimensions={0} | all-to-all | bytes 2097152 | tf_op jit(solution)/shard_map/all_to_all | solution.py:200
  74.9 1.8 %shard_map.101.refs_3_ = f32[136,1024]{1,0:T(8,128)S(1)} custom-call(s32[1]{0:T(128)} %bitcast.sp_ref.refs_0_, bf16[4,128,1024]{2,1,0:T(8,128)(2,1)S(1)} %all_to_all.15.refs_1_, bf16[16,2,128,128]{3,2,1,0:T(8,128)(2,1)S(1)} %bitcast.7), custom_call_target="tpu_custom_call" | custom-call | flops 1073741824 | bytes 1048576 | tf_op jit(solution)/shard_map/pallas_call | solution.py:49
  76.7 3.5 %shard_map.103 = bf16[136,1024]{1,0:T(8,128)(2,1)S(1)} custom-call(s32[1]{0:T(128)} %bitcast.sp_ref.refs_0_, bf16[4,128,1024]{2,1,0:T(8,128)(2,1)S(1)} %all_to_all.15.refs_1_, bf16[16,2,128,128]{3,2,1,0:T(8,128)(2,1)S(1)} %bitcast.8, bf16[16,2,128,128]{3,2,1,0:T(8,128)(2,1)S(1)} %collective-permute-done.refs_3_.refs_2_), custom_call_target="tpu_custom_call" | custom-call | flops 2147483648 | bytes 1048576 | tf_op jit(solution)/shard_map/pallas_call | solution.py:49
  80.3 2.7 %collective-permute-start.2 = (bf16[136,1024]{1,0:T(8,128)(2,1)S(1)}, bf16[136,1024]{1,0:T(8,128)(2,1)S(1)}, u32[]{:S(2)}, u32[]{:S(2)}) collective-permute-start(bf16[136,1024]{1,0:T(8,128)(2,1)S(1)} %shard_map.103), channel_id=1, source_target_pairs={{0,16},{4,20},{8,24},{12,28},{16,0},{20,4},{24,8},{28,12},{1,17},{... | collective-permute-start | bytes 835592 | tf_op jit(solution)/shard_map/ppermute | solution.py:208
  83.0 3.6 %shard_map.104 = bf16[136,1024]{1,0:T(8,128)(2,1)S(1)} custom-call(s32[1]{0:T(128)} %bitcast.sp_ref.refs_0_, bf16[4,128,1024]{2,1,0:T(8,128)(2,1)S(1)} %all_to_all.15.refs_1_, bf16[16,2,128,128]{3,2,1,0:T(8,128)(2,1)S(1)} %bitcast.9, bf16[16,2,128,128]{3,2,1,0:T(8,128)(2,1)S(1)} %collective-permute-done.refs_3_.refs_2_), custom_call_target="tpu_custom_call" | custom-call | flops 2147483648 | bytes 1048576 | tf_op jit(solution)/shard_map/pallas_call | solution.py:49
  86.6 4.5 %collective-permute-start.3 = (bf16[136,1024]{1,0:T(8,128)(2,1)S(1)}, bf16[136,1024]{1,0:T(8,128)(2,1)S(1)}, u32[]{:S(2)}, u32[]{:S(2)}) collective-permute-start(bf16[136,1024]{1,0:T(8,128)(2,1)S(1)} %shard_map.104), channel_id=1, source_target_pairs={{0,24},{4,12},{8,0},{12,20},{16,8},{20,28},{24,16},{28,4},{1,25},{... | collective-permute-start | bytes 835592 | tf_op jit(solution)/shard_map/ppermute | solution.py:208
  91.1 1.9 %shard_map.102 = bf16[136,1024]{1,0:T(8,128)(2,1)S(1)} custom-call(s32[1]{0:T(128)} %bitcast.sp_ref.refs_0_, bf16[4,128,1024]{2,1,0:T(8,128)(2,1)S(1)} %all_to_all.15.refs_1_, bf16[16,2,128,128]{3,2,1,0:T(8,128)(2,1)S(1)} %collective-permute-done.refs_3_.refs_2_, f32[136,1024]{1,0:T(8,128)S(1)} %shard_map.101.refs_3_), custom_call_target="tpu_custom_call" | custom-call | flops 1073741824 | bytes 1048576 | tf_op jit(solution)/shard_map/pallas_call | solution.py:49
  93.0 2.1 %collective-permute-start.1 = (bf16[136,1024]{1,0:T(8,128)(2,1)S(1)}, bf16[136,1024]{1,0:T(8,128)(2,1)S(1)}, u32[]{:S(2)}, u32[]{:S(2)}) collective-permute-start(bf16[136,1024]{1,0:T(8,128)(2,1)S(1)} %shard_map.102), channel_id=1, source_target_pairs={{0,8},{4,28},{8,16},{12,4},{16,24},{20,12},{24,0},{28,20},{1,9},{5... | collective-permute-start | bytes 835592 | tf_op jit(solution)/shard_map/ppermute | solution.py:208
  95.0 3.5 %shard_map.100.own_ref = f32[136,1024]{1,0:T(8,128)S(1)} custom-call(s32[1]{0:T(128)} %bitcast.sp_ref.refs_0_, bf16[4,128,1024]{2,1,0:T(8,128)(2,1)S(1)} %all_to_all.15.refs_1_, bf16[16,2,128,128]{3,2,1,0:T(8,128)(2,1)S(1)} %bitcast.10, bf16[16,2,128,128]{3,2,1,0:T(8,128)(2,1)S(1)} %collective-permute-done.refs_3_.refs_2_), custom_call_target="tpu_custom_call" | custom-call | flops 2147483648 | bytes 1048576 | tf_op jit(solution)/shard_map/pallas_call | solution.py:49
  98.6 4.2 %collective-permute-done.1.refs_0_ = bf16[136,1024]{1,0:T(8,128)(2,1)S(1)} collective-permute-done((bf16[136,1024]{1,0:T(8,128)(2,1)S(1)}, bf16[136,1024]{1,0:T(8,128)(2,1)S(1)}, u32[]{:S(2)}, u32[]{:S(2)}) %collective-permute-start.1) | collective-permute-done | bytes 278560 | tf_op jit(solution)/shard_map/ppermute | solution.py:208
  102.8 0.5 shard_map.105
  103.3 9.1 %all_to_all.16.part_ref = bf16[4,32,1024]{2,1,0:T(8,128)(2,1)S(1)} all-to-all(bf16[4,32,1024]{2,1,0:T(8,128)(2,1)S(1)} %bitcast.4), channel_id=1, replica_groups=mesh['z'=16,'x'=4,'c'=2,'y'=4] {'y'}, dimensions={0} | all-to-all | bytes 524288 | tf_op jit(solution)/shard_map/all_to_all | solution.py:218
  112.4 0.7 shard_map.106
  (10 shorter events, 0.0 us)
Async XLA Ops:
  1.6 11.2 %all-to-all-start = ((bf16[4,32,1024]{2,1,0:T(8,128)(2,1)}), bf16[4,32,1024]{2,1,0:T(8,128)(2,1)S(1)}, u32[]{:S(2)}, u32[]{:S(2)}) async-start(bf16[4,32,1024]{2,1,0:T(8,128)(2,1)} %spread.1), calls=%async_computation | async-start | bytes 524288 | tf_op jit(solution)/shard_map/all_to_all | solution.py:188
  6.8 5.9 %copy-start.1 = (f32[2,256,128]{2,1,0:T(8,128)S(1)}, f32[2,256,128]{2,1,0:T(8,128)}, u32[]{:S(2)}) copy-start(f32[2,256,128]{2,1,0:T(8,128)} %constant.24.clone.rows_ref) | copy-start | bytes 786436
  6.8 5.9 %copy-start.2 = (f32[2,64,128]{2,1,0:T(8,128)S(1)}, f32[2,64,128]{2,1,0:T(8,128)}, u32[]{:S(2)}) copy-start(f32[2,64,128]{2,1,0:T(8,128)} %constant.25.clone.cols_ref) | copy-start | bytes 196612
  53.0 23.7 %collective-permute-start = (bf16[16,2,128,128]{3,2,1,0:T(8,128)(2,1)S(1)}, bf16[16,2,128,128]{3,2,1,0:T(8,128)(2,1)S(1)}, u32[]{:S(2)}, u32[]{:S(2)}) collective-permute-start(bf16[16,2,128,128]{3,2,1,0:T(8,128)(2,1)S(1)} %bitcast.6), channel_id=1, source_target_pairs={{0,4},{4,0},{1,5},{5,1},{2,6},{6,2},{3,7},{7,3},{8,12},{12,8},{9,1... | collective-permute-start | bytes 3145736 | tf_op jit(solution)/shard_map/ppermute | solution.py:204
  80.3 18.3 %collective-permute-start.2 = (bf16[136,1024]{1,0:T(8,128)(2,1)S(1)}, bf16[136,1024]{1,0:T(8,128)(2,1)S(1)}, u32[]{:S(2)}, u32[]{:S(2)}) collective-permute-start(bf16[136,1024]{1,0:T(8,128)(2,1)S(1)} %shard_map.103), channel_id=1, source_target_pairs={{0,16},{4,20},{8,24},{12,28},{16,0},{20,4},{24,8},{28,12},{1,17},{... | collective-permute-start | bytes 835592 | tf_op jit(solution)/shard_map/ppermute | solution.py:208
  86.6 12.0 %collective-permute-start.3 = (bf16[136,1024]{1,0:T(8,128)(2,1)S(1)}, bf16[136,1024]{1,0:T(8,128)(2,1)S(1)}, u32[]{:S(2)}, u32[]{:S(2)}) collective-permute-start(bf16[136,1024]{1,0:T(8,128)(2,1)S(1)} %shard_map.104), channel_id=1, source_target_pairs={{0,24},{4,12},{8,0},{12,20},{16,8},{20,28},{24,16},{28,4},{1,25},{... | collective-permute-start | bytes 835592 | tf_op jit(solution)/shard_map/ppermute | solution.py:208
  93.0 9.8 %copy-start = (bf16[1024,1024]{1,0:T(8,128)(2,1)S(1)}, bf16[1024,1024]{1,0:T(8,128)(2,1)}, u32[]{:S(2)}) copy-start(bf16[1024,1024]{1,0:T(8,128)(2,1)} %refs_3_.1) | copy-start | bytes 6291460
  93.0 9.8 %collective-permute-start.1 = (bf16[136,1024]{1,0:T(8,128)(2,1)S(1)}, bf16[136,1024]{1,0:T(8,128)(2,1)S(1)}, u32[]{:S(2)}, u32[]{:S(2)}) collective-permute-start(bf16[136,1024]{1,0:T(8,128)(2,1)S(1)} %shard_map.102), channel_id=1, source_target_pairs={{0,8},{4,28},{8,16},{12,4},{16,24},{20,12},{24,0},{28,20},{1,9},{5... | collective-permute-start | bytes 835592 | tf_op jit(solution)/shard_map/ppermute | solution.py:208
